TPU v7x, 256 devices: a whole 4x4x8 slice. The times are simulated.
256 devices in a mesh: fs: 64 (over z, x, core), tp: 4 (over y).
Axes of the slice: x: 4, y: 4, z: 8, core: 2. Of those that a mesh axis runs over, the one named last changes fastest.
Arguments:
- tokens: bfloat16 [768, 4, 2048], P(None, 'tp'), may hold values from -6 to 6
- norm_gain: float32 [2048], P('fs'), may hold values from 0.1 to 1.9
- gate_weight: float32 [8, 2048, 4096], P(None, 'fs', 'tp'), may hold values from -0.125 to 0.125
- up_weight: float32 [8, 2048, 4096], P(None, 'fs', 'tp'), may hold values from -0.125 to 0.125
- down_weight: float32 [8, 2048, 4096], P(None, 'fs', 'tp'), may hold values from -0.09375 to 0.09375
- expert_ids: int32 [768, 4, 2], P(None, 'tp'), may hold values from 0 to 7, all different within a row
- expert_mix: float32 [768, 4, 2], P(None, 'tp'), may hold values from 0.2 to 1
Outputs:
- gate_serve: bfloat16 [8, 2048, 4096], P(None, None, 'fs')
- up_serve: bfloat16 [8, 2048, 4096], P(None, None, 'fs')
- down_serve: bfloat16 [8, 2048, 4096], P(None, None, 'fs')
- mixed: bfloat16 [768, 4, 2048], P('fs', 'tp')
Inputs may be any that keep to these rules, and one draw needn't show every extreme that they name: `expert_ids`: each token names two different experts.
All inputs are finite; a program needn't handle non-finite values.
Results may differ from a plain program's by a relative error of at most 0.0082.
Values may be sent and summed in bfloat16 or wider, within the bound.
A program may use at most 64 MiB of HBM per device.

v0:
```python
import jax
import jax.numpy as jnp
from jax import lax
from jax.sharding import Mesh
from jax.sharding import PartitionSpec as P

FS = ("fs_0", "fs_1", "fs_2")


norm_eps = 1e-05


def sent_together(arrays, axis, split_dim, concat_dim, along):
    ends, at = ([], 0)
    for a in arrays[:-1]:
        at += a.shape[along]
        ends.append(at)
    both = jnp.concatenate(arrays, axis=along)
    return tuple(
        jnp.split(
            lax.all_to_all(both, axis, split_axis=split_dim, concat_axis=concat_dim, tiled=True),
            ends,
            axis=along,
        )
    )


def sent_together_2(arrays, axis, dim, along):
    both = jnp.concatenate(arrays, axis=along)
    result, at, gathered = (lax.all_gather(both, axis, axis=dim, tiled=True), 0, [])
    for a in arrays:
        gathered.append(lax.slice_in_dim(result, at, at + a.shape[along], axis=along))
        at += a.shape[along]
    return tuple(gathered)


def summed_rows(so_far, axes):
    for axis in axes:
        so_far = lax.psum_scatter(so_far, axis, scatter_dimension=0, tiled=True)
    return so_far


def local(tokens, norm_gain, gate_weight, up_weight, down_weight, expert_ids, expert_mix):
    gate_folded = (gate_weight * norm_gain[None, :, None]).astype(jnp.bfloat16)
    up_folded = (up_weight * norm_gain[None, :, None]).astype(jnp.bfloat16)
    down_cast = down_weight.astype(jnp.bfloat16)
    regrouped = sent_together((gate_folded, up_folded, down_cast), "tp", 0, 2, 1)
    unit_split = sent_together((regrouped[0], regrouped[1], regrouped[2]), FS, 2, 1, 0)
    gate_serve, up_serve, down_serve = sent_together_2(
        (unit_split[0], unit_split[1], unit_split[2]), "tp", 0, 1
    )
    width = tokens.shape[2]
    token_rows = tokens.reshape(-1, width).astype(jnp.float32)
    row_mean = jnp.mean(token_rows, axis=1, keepdims=True)
    centered = token_rows - row_mean
    variance = jnp.mean(centered * centered, axis=1, keepdims=True)
    normed = (centered * lax.rsqrt(variance + norm_eps)).astype(jnp.bfloat16)
    route_ids = expert_ids.reshape(-1, 2)
    route_mix = expert_mix.reshape(-1, 2)
    expert_iota = jnp.arange(gate_serve.shape[0], dtype=jnp.int32)
    expert_gates = jnp.sum(
        (route_ids[:, :, None] == expert_iota[None, None, :]).astype(jnp.float32)
        * route_mix[:, :, None],
        axis=1,
    )
    gate_act = jnp.einsum("rd,edf->ref", normed, gate_serve, preferred_element_type=jnp.float32)
    up_act = jnp.einsum("rd,edf->ref", normed, up_serve, preferred_element_type=jnp.float32)
    hidden = (jax.nn.silu(gate_act) * up_act * expert_gates[:, :, None]).astype(jnp.bfloat16)
    own_rows = token_rows.shape[0] // lax.axis_size(FS)
    summed = summed_rows(
        jnp.einsum("ref,edf->rd", hidden, down_serve, preferred_element_type=jnp.float32), FS
    )
    mixed = summed.astype(jnp.bfloat16).reshape(own_rows, 1, width)
    return (gate_serve, up_serve, down_serve, mixed)


def solution(mesh):
    finer = Mesh(mesh.devices.reshape(8, 4, 2, mesh.shape["tp"]), ("fs_0", "fs_1", "fs_2", "tp"))
    placed = (
        P(None, "tp", None),
        P(FS),
        P(None, FS, "tp"),
        P(None, FS, "tp"),
        P(None, FS, "tp"),
        P(None, "tp", None),
        P(None, "tp", None),
    )
    return jax.shard_map(
        local,
        mesh=finer,
        in_specs=placed,
        out_specs=(P(None, None, FS), P(None, None, FS), P(None, None, FS), P(FS, "tp", None)),
        check_vma=False,
    )
```

profile of v0, /device:TPU:1, one launch (start us, length us, event | category | flops | bytes accessed | tf_op | source)
XLA Modules:
  0.0 326.5 jit_solution(13660195549617188783)
XLA Ops:
  7.2 1.4 convert_element_type.27
  8.7 1.5 multiply_convert_fusion.2
  10.4 24.7 %all_to_all.33 = bf16[8,96,1024]{2,1,0:T(8,128)(2,1)S(1)} all-to-all(bf16[8,96,1024]{2,1,0:T(8,128)(2,1)S(1)} %pad_maximum_fusion.1), channel_id=1, replica_groups=mesh['fs_0'=8,'fs_1'=4,'fs_2'=2,'tp'=4] {'tp'}, dimensions={0} | all-to-all | bytes 3145728 | tf_op jit(solution)/shard_map/all_to_all | solution.py:21
  35.0 1.2 copy.40
  36.3 1.2 all_to_all.27
  37.8 7.3 %copy.32 = bf16[6,32,4096]{1,0,2:T(8,128)(2,1)} copy(bf16[6,32,4096]{2,1,0:T(8,128)(2,1)S(1)} %pad_maximum_fusion.2) | data formatting | bytes 3145728 | tf_op jit(solution)/shard_map/concatenate | solution.py:18
  45.1 10.7 %reshape.39 = bf16[64,2,6144]{2,1,0:T(2,128)(2,1)S(1)} reshape(bf16[4096,6,32]{2,1,0:T(8,128)(2,1)} %bitcast.45) | data formatting | bytes 3145728
  55.8 52.1 %all_to_all.34 = bf16[64,2,6144]{2,1,0:T(2,128)(2,1)S(1)} all-to-all(bf16[64,2,6144]{2,1,0:T(2,128)(2,1)S(1)} %reshape.39), channel_id=1, replica_groups=mesh['fs_0'=8,'fs_1'=4,'fs_2'=2,'tp'=4] {'fs_0','fs_1','fs_2'}, dimensions={0} | all-to-all | bytes 3145728 | tf_op jit(solution)/shard_map/all_to_all | solution.py:21
  108.0 7.6 %reshape.40 = bf16[4096,6,32]{2,1,0:T(8,128)(2,1)} reshape(bf16[64,2,6144]{2,1,0:T(2,128)(2,1)S(1)} %all_to_all.34) | data formatting | bytes 3145728
  115.5 8.6 %copy.38 = bf16[6,32,64,64]{3,2,1,0:T(8,128)(2,1)S(1)} copy(bf16[6,32,64,64]{1,0,3,2:T(8,128)(2,1)} %bitcast.46) | data formatting | bytes 3145728 | tf_op jit(solution)/shard_map/all_to_all | solution.py:21
  124.1 0.7 fusion.15
  124.8 0.7 copy.34
  126.9 2.0 pad_maximum_fusion
  128.9 4.4 %copy.37 = bf16[2,6144,64]{1,2,0:T(8,128)(2,1)} copy(bf16[2,6144,64]{2,1,0:T(8,128)(2,1)} %pad_maximum_fusion) | data formatting | bytes 3145728 | tf_op jit(solution)/shard_map/concatenate | solution.py:29
  134.1 1.0 fusion.4
  135.0 61.6 %all-gather.2.cloned.1.call-done = bf16[8,6144,64]{1,2,0:T(8,128)(2,1)} async-done(((bf16[2,6144,64]{1,2,0:T(8,128)(2,1)}), bf16[8,6144,64]{1,2,0:T(8,128)(2,1)}) %all-gather.2.cloned.1.call-update) | async-done | bytes 6291472 | tf_op jit(solution)/shard_map/all_gather | solution.py:30
  196.7 4.0 %fusion.14 = (bf16[8,2048,64]{1,2,0:T(8,128)(2,1)S(1)}, bf16[8,2048,64]{1,2,0:T(8,128)(2,1)S(1)}, bf16[8,2048,64]{1,2,0:T(8,128)(2,1)S(1)}) fusion(bf16[8,6144,64]{1,2,0:T(8,128)(2,1)} %all-gather.2.cloned.1.call-done), kind=kLoop, calls=%fused_computation.26 | loop fusion | bytes 12582912 | tf_op jit(solution)/shard_map/slice | solution.py:32
  200.7 1.9 fusion.12
  202.7 1.9 fusion.10
  204.6 4.6 %convolution_bitcast_fusion = f32[768,2048]{1,0:T(8,128)} fusion(bf16[8,2048,64]{1,2,0:T(8,128)(2,1)S(1)} %get-tuple-element.4, f32[768,8,64]{0,2,1:T(8,128)S(1)} %bitcast.58, f32[768,8,64]{0,2,1:T(8,128)S(1)} %bitcast.57, f32[768,8]{0,1:T(8,128)S(1)} %select_reduce_fusion), kind=kOutput, calls=%fused_computation.7 | convolution fusion | flops 1613365248 | bytes 11558912 | tf_op jit(solution)/shard_map/ref,edf->rd/dot_general | solution.py:71
  209.2 76.0 %reduce-scatter.5.cloned.1.call-done = f32[96,2048]{1,0:T(8,128)} async-done(((f32[768,2048]{1,0:T(8,128)}), f32[96,2048]{1,0:T(8,128)}) %reduce-scatter.5.cloned.1.call-update) | async-done | bytes 786448 | tf_op jit(solution)/shard_map/reduce_scatter | solution.py:39
  285.3 24.2 %reduce-scatter.7.cloned.1.call-done = f32[24,2048]{1,0:T(8,128)} async-done(((f32[96,2048]{1,0:T(8,128)}), f32[24,2048]{1,0:T(8,128)}) %reduce-scatter.7.cloned.1.call-update) | async-done | bytes 196624 | tf_op jit(solution)/shard_map/reduce_scatter | solution.py:39
  309.5 6.5 %fusion = f32[16,2048]{1,0:T(8,128)S(1)} fusion(f32[24,2048]{1,0:T(8,128)} %reduce-scatter.7.cloned.1.call-done), kind=kCustom, calls=%all-reduce-scatter | all-reduce-scatter fusion | flops 65537 | bytes 328704
  316.0 1.3 collective-permute-start
  (36 shorter events, 4.8 us)
Async XLA Ops:
  7.2 1.5 copy-start.4
  7.2 189.5 %all-gather.2.cloned.1.call-start = ((), (), s32[]{:S(2)}) async-start(), calls=%async_computation.4 | async-start | bytes 7864320 | tf_op jit(solution)/shard_map/all_gather | solution.py:30
  128.8 4.7 %copy-start.5 = (f32[768,1,2]{0,2,1:T(2,128)S(1)}, f32[768,1,2]{0,2,1:T(2,128)}, u32[]{:S(2)}) copy-start(f32[768,1,2]{0,2,1:T(2,128)} %param.13) | copy-start | bytes 18436
  128.8 4.7 %copy-start.6 = (s32[768,1,2]{0,2,1:T(2,128)S(1)}, s32[768,1,2]{0,2,1:T(2,128)}, u32[]{:S(2)}) copy-start(s32[768,1,2]{0,2,1:T(2,128)} %param.12) | copy-start | bytes 18436
  128.8 4.7 %copy-start = (bf16[768,1,2048]{2,0,1:T(8,128)(2,1)S(1)}, bf16[768,1,2048]{2,0,1:T(8,128)(2,1)}, u32[]{:S(2)}) copy-start(bf16[768,1,2048]{2,0,1:T(8,128)(2,1)} %param.7) | copy-start | bytes 9437188
  133.3 151.9 %reduce-scatter.5.cloned.1.call-start = ((), (), s32[]{:S(2)}) async-start(), calls=%async_computation.5 | async-start | bytes 7077888 | tf_op jit(solution)/shard_map/reduce_scatter | solution.py:39
  200.7 1.9 copy-start.3
  200.7 2.0 copy-start.2
  200.7 3.9 %copy-start.1 = (bf16[8,2048,64]{1,2,0:T(8,128)(2,1)}, bf16[8,2048,64]{1,2,0:T(8,128)(2,1)S(1)}, u32[]{:S(2)}) copy-start(bf16[8,2048,64]{1,2,0:T(8,128)(2,1)S(1)} %get-tuple-element.4) | copy-start | bytes 6291460
  209.2 108.1 %copy-start.7 = (u32[256]{0:T(256)S(1)}, u32[256]{0:T(256)}, u32[]{:S(2)}) copy-start(u32[256]{0:T(256)} %constant.21) | copy-start | bytes 3076
  209.2 100.3 %reduce-scatter.7.cloned.1.call-start = ((), (), s32[]{:S(2)}) async-start(), calls=%async_computation.6 | async-start | bytes 983040 | tf_op jit(solution)/shard_map/reduce_scatter | solution.py:39
  316.0 3.1 collective-permute-start
Sparse Core Ops, SparseCore 0:
  133.4 63.2 all-gather.1
  209.3 75.8 reduce-scatter.4
  287.8 21.6 reduce-scatter.6
where the time goes:
time: 327 us; the launch traced here: 326 us
  waiting for transfers between devices  162 us (50%)
  blocking collectives  83.3 us (25%)
  local copies, waits for them, and re-layouts  49.5 us (15%)
  between operations  14.6 us (4%)
  matrix products  8.38 us (3%)
  other arithmetic  6.63 us (2%)
    reduce_scatter x2, waiting for transfers between devices, summed_rows(): so_far = lax.psum_scatter(so_far, axis, scatter_dimension=0, tiled=True)  100 us
    all_to_all x2, blocking collectives, sent_together(): lax.all_to_all(both, axis, split_axis=split_dim, concat_axis=concat_dim,...  76.8 us
    all_gather x1, waiting for transfers between devices, sent_together_2(): lax.all_gather(both, axis, axis=dim, tiled=True)  61.6 us
    unnamed x21, local copies, waits for them, and re-layouts  19.3 us
    all_to_all x3, local copies, waits for them, and re-layouts, sent_together(): lax.all_to_all(both, axis, split_axis=split_dim, concat_axis=concat_dim,...  11 us
    concatenate x1, local copies, waits for them, and re-layouts, sent_together(): both = jnp.concatenate(arrays, axis=along)  7.33 us
  transfers between devices with their start and end apart: 4, of which 4 were waited for; matrix products, arithmetic and copies ran while one was open for 1% of the time, Pallas kernels for 0%

commit v1 on v0

v1 whole, which is shorter than its diff:
```python
import jax
import jax.numpy as jnp
from jax import lax
from jax.experimental import pallas as pl
from jax.experimental.pallas import tpu as pltpu
from jax.sharding import Mesh
from jax.sharding import PartitionSpec as P

FS = ("fs_0", "fs_1", "fs_2")
NZ, NX, NC, NY = 8, 4, 2, 4
norm_eps = 1e-05
BF, F32 = jnp.bfloat16, jnp.float32
MESH = pl.DeviceIdType.MESH

CHUNKS = ((0, 0), (1, 0), (0, 1), (1, 1), (2, 0), (2, 1))
NQ = len(CHUNKS)


def send(src, dst, send_sem, recv_sem, to):
    pltpu.make_async_remote_copy(
        src_ref=src, dst_ref=dst, send_sem=send_sem, recv_sem=recv_sem, device_id=to, device_id_type=MESH
    ).start()


def wait_bytes(ref, sem):
    pltpu.make_async_copy(ref, ref, sem).wait()


def greet(z, x, c, y, along_y):
    barrier = pltpu.get_barrier_semaphore()
    count = 0
    me = 2 * x + c
    for off in range(1, NX * NC):
        j = lax.rem(me + off, NX * NC)
        pl.semaphore_signal(
            barrier, inc=1, device_id={"fs_1": j // 2, "fs_2": lax.rem(j, 2)}, device_id_type=MESH
        )
        count += 1
    for off in range(1, NZ):
        pl.semaphore_signal(barrier, inc=1, device_id={"fs_0": lax.rem(z + off, NZ)}, device_id_type=MESH)
        count += 1
    if along_y:
        for off in (1, NY - 1):
            pl.semaphore_signal(barrier, inc=1, device_id={"tp": lax.rem(y + off, NY)}, device_id_type=MESH)
            count += 1
    pl.semaphore_wait(barrier, count)


def weights_kernel(
    gate, up, down, gain, og, ou, od,
    xs, xr, ts, az, fw, w,
    x_send, x_recv, a_send, a_recv, f_send, f_recv, z_send, z_recv, c_send, c_recv, g_send, g_recv, o_sem,
):
    z, x, c, y = (lax.axis_index(a) for a in ("fs_0", "fs_1", "fs_2", "tp"))
    me = 2 * x + c
    ahead, behind, across = (lax.rem(y + o, NY) for o in (1, 3, 2))
    mats, outs = (gate, up, down), (og, ou, od)
    column = pl.multiple_of(256 * z, 256)
    greet(z, x, c, y, True)

    def pack(q):
        m, el = CHUNKS[q]
        low = lax.broadcasted_iota(jnp.int32, (32, 128), 1) < 64

        def one(i, carry):
            ep, xp = i // NX, lax.rem(i, NX)
            left = pl.multiple_of(128 * xp, 128)
            a = mats[m][2 * ep + el, :, pl.ds(left, 128)]
            b = mats[m][2 * ep + el, :, pl.ds(pl.multiple_of(512 + left, 128), 128)]
            if m < 2:
                a, b = a * gain[...], b * gain[...]
            xs[q, 2 * xp, ep] = jnp.where(low, a, pltpu.roll(b, 64, 1)).astype(BF)
            xs[q, 2 * xp + 1, ep] = jnp.where(low, pltpu.roll(a, 64, 1), b).astype(BF)
            return carry

        lax.fori_loop(0, 4 * NX, one, 0)
        for off in range(1, NX * NC):
            j = lax.rem(me + off, NX * NC)
            send(
                xs.at[q, j], xr.at[q, me], x_send.at[q], x_recv.at[q],
                {"fs_1": j // 2, "fs_2": lax.rem(j, 2)},
            )
        xr[q, me] = xs[q, me]

    def turn(q):
        wait_bytes(xr.at[q, 0:7], x_recv.at[q])

        def one(ep, carry):
            for h in range(2):
                rows = jnp.concatenate([xr[q, 4 * h + k, ep] for k in range(4)], axis=0)
                ts[q, ep, :, 128 * h : 128 * (h + 1)] = rows.T
            return carry

        lax.fori_loop(0, 4, one, 0)
        send(ts.at[q, across, 0:64], fw.at[q, 0], a_send.at[q], f_recv.at[q, 0], {"tp": ahead})
        send(ts.at[q, across, 64:128], fw.at[q, 1], a_send.at[q], f_recv.at[q, 1], {"tp": behind})
        send(ts.at[q, ahead], az.at[q, y], a_send.at[q], a_recv.at[q], {"tp": ahead})
        send(ts.at[q, behind], az.at[q, y], a_send.at[q], a_recv.at[q], {"tp": behind})
        az[q, y] = ts[q, y]

    def relay(q):
        wait_bytes(fw.at[q, 0], f_recv.at[q, 0])
        send(fw.at[q, 0], az.at[q, behind, 0:64], f_send.at[q], a_recv.at[q], {"tp": ahead})
        wait_bytes(fw.at[q, 1], f_recv.at[q, 1])
        send(fw.at[q, 1], az.at[q, ahead, 64:128], f_send.at[q], a_recv.at[q], {"tp": behind})

    def along_z(q):
        wait_bytes(az.at[q, 0:3], a_recv.at[q])
        for off in (4, 3, 5, 2, 6, 1, 7):
            zp = lax.rem(z + off, NZ)
            rows = pl.multiple_of(64 * lax.rem(zp, 2), 64)
            send(
                az.at[q, zp // 2, pl.ds(rows, 64), :], w.at[q, y, :, pl.ds(column, 256)],
                z_send.at[q], z_recv.at[q], {"fs_0": zp},
            )
        rows = pl.multiple_of(64 * lax.rem(z, 2), 64)
        w[q, y, :, pl.ds(column, 256)] = az[q, z // 2, pl.ds(rows, 64), :]

    def spread(q):
        wait_bytes(w.at[q, 0, :, 0:1792], z_recv.at[q])
        send(w.at[q, y], w.at[q, y], c_send.at[q], c_recv.at[q, 0], {"tp": ahead})
        send(w.at[q, y], w.at[q, y], c_send.at[q], c_recv.at[q, 1], {"tp": behind})

    def spread_on(q):
        wait_bytes(w.at[q, behind], c_recv.at[q, 0])
        send(w.at[q, behind, 0:32], w.at[q, behind, 0:32], g_send.at[q], g_recv.at[q], {"tp": ahead})
        wait_bytes(w.at[q, ahead], c_recv.at[q, 1])
        send(w.at[q, ahead, 32:64], w.at[q, ahead, 32:64], g_send.at[q], g_recv.at[q], {"tp": behind})

    def put_out(q):
        m, el = CHUNKS[q]
        wait_bytes(w.at[q, across], g_recv.at[q])
        for ep in range(4):
            pltpu.make_async_copy(w.at[q, ep], outs[m].at[2 * ep + el], o_sem.at[q]).start()

    stages = (pack, turn, relay, along_z, spread, spread_on, put_out)
    for q in range(NQ):
        pack(q)
    order = []
    for q in range(NQ):
        order += [(2.8 * q + 5, 1, q), (2.8 * q + 9, 2, q), (2.8 * q + 12, 3, q), (max(5.6 * q + 20, 8.5 * q + 18), 4, q)]
        order += [(11.2 * q + 32, 5, q), (11.2 * q + 40, 6, q)]
    for _, s, q in sorted(order):
        stages[s](q)
    for q in range(NQ):
        wait_bytes(xr.at[q, 0:7], x_send.at[q])
        wait_bytes(az.at[q, 0:3], a_send.at[q])
        wait_bytes(az.at[q, 0], f_send.at[q])
        wait_bytes(w.at[q, 0, :, 0:1792], z_send.at[q])
        wait_bytes(w.at[q, 0:2], c_send.at[q])
        wait_bytes(w.at[q, 0], g_send.at[q])
        wait_bytes(w.at[q], o_sem.at[q])


def move_weights(gate, up, down, gain):
    out = jax.ShapeDtypeStruct((8, 64, 2048), BF)
    vmem = pl.BlockSpec(memory_space=pltpu.VMEM)
    hbm = pl.BlockSpec(memory_space=pl.ANY)
    dma = pltpu.SemaphoreType.DMA
    return pl.pallas_call(
        weights_kernel,
        out_shape=(out, out, out),
        in_specs=[vmem] * 4,
        out_specs=(hbm, hbm, hbm),
        scratch_shapes=[
            pltpu.VMEM((NQ, 8, 4, 32, 128), BF),
            pltpu.VMEM((NQ, 8, 4, 32, 128), BF),
            pltpu.VMEM((NQ, 4, 128, 256), BF),
            pltpu.VMEM((NQ, 4, 128, 256), BF),
            pltpu.VMEM((NQ, 2, 64, 256), BF),
            pltpu.VMEM((NQ, 4, 64, 2048), BF),
            dma((NQ,)), dma((NQ,)),
            dma((NQ,)), dma((NQ,)),
            dma((NQ,)), dma((NQ, 2)),
            dma((NQ,)), dma((NQ,)),
            dma((NQ,)), dma((NQ, 2)),
            dma((NQ,)), dma((NQ,)),
            dma((NQ,)),
        ],
        compiler_params=pltpu.CompilerParams(
            collective_id=0, has_side_effects=True, vmem_limit_bytes=40 * 1024 * 1024
        ),
        name="move_weights",
    )(gate, up, down, gain)


BLOCK = 96
OFFSETS = (4, 3, 5, 2, 6, 1, 7, 0)


def sum_kernel(
    p, out, r1, s1, r2, s2, r3, s4, r4,
    send1, recv1, send2, recv2, send3, recv3, send4, recv4,
):
    z, x, c, y = (lax.axis_index(a) for a in ("fs_0", "fs_1", "fs_2", "tp"))
    mine, theirs = pl.multiple_of(1024 * c, 1024), pl.multiple_of(1024 * (1 - c), 1024)
    greet(z, x, c, y, False)

    def rows_of(k):
        zp = lax.rem(z + OFFSETS[k], NZ)
        return zp, pl.ds(pl.multiple_of(BLOCK * zp, BLOCK), BLOCK)

    def between_cores(k):
        _, rows = rows_of(k)
        send(p.at[rows, pl.ds(theirs, 1024)], r1.at[k], send1.at[k], recv1.at[k], {"fs_2": 1 - c})

    def along_x(k):
        _, rows = rows_of(k)
        wait_bytes(r1.at[k], recv1.at[k])
        total = p[rows, pl.ds(mine, 1024)].astype(F32) + r1[k].astype(F32)
        total = total.astype(BF)
        for xp in range(NX):
            s1[k, xp] = total[:, 256 * xp : 256 * (xp + 1)]
        for off in (2, 1, 3):
            xp = lax.rem(x + off, NX)
            send(s1.at[k, xp], r2.at[k, x], send2.at[k], recv2.at[k], {"fs_1": xp})
        r2[k, x] = s1[k, x]

    def along_z(k):
        zp, _ = rows_of(k)
        wait_bytes(r2.at[k, 0:3], recv2.at[k])
        total = (r2[k, 0].astype(F32) + r2[k, 1].astype(F32)) + (r2[k, 2].astype(F32) + r2[k, 3].astype(F32))
        if OFFSETS[k] == 0:
            r3[z] = total.astype(BF)
        else:
            s2[k] = total.astype(BF)
            send(s2.at[k], r3.at[z], send3.at[k], recv3, {"fs_0": zp})

    for k in range(NZ):
        between_cores(k)
    for k in range(NZ + 1):
        if k < NZ:
            along_x(k)
        if k > 0:
            along_z(k - 1)
    wait_bytes(r3.at[0:7], recv3)
    total = r3[0].astype(F32)
    for i in range(1, NZ):
        total = total + r3[i].astype(F32)
    row = lax.broadcasted_iota(jnp.int32, (128, BLOCK), 0)
    col = lax.broadcasted_iota(jnp.int32, (128, BLOCK), 1)
    within = lax.rem(row, 16)
    pick = ((col == (row // 16) * 12 + within) & (within < 12)).astype(BF)
    s4[...] = jnp.dot(pick, total.astype(BF), preferred_element_type=F32).astype(BF)
    me = 2 * x + c
    column = pl.multiple_of(256 * (4 * c + x), 256)
    for off in range(1, NX * NC):
        j = lax.rem(me + off, NX * NC)
        send(
            s4.at[pl.ds(pl.multiple_of(16 * j, 16), 16), :], r4.at[:, pl.ds(column, 256)],
            send4, recv4, {"fs_1": j // 2, "fs_2": lax.rem(j, 2)},
        )
    r4[:, pl.ds(column, 256)] = s4[pl.ds(pl.multiple_of(16 * me, 16), 16), :]
    wait_bytes(r4.at[:, 0:1792], recv4)
    out[...] = r4[0:12, :]
    for k in range(NZ):
        wait_bytes(r1.at[k], send1.at[k])
        wait_bytes(r2.at[k, 0:3], send2.at[k])
        if OFFSETS[k] != 0:
            wait_bytes(s2.at[k], send3.at[k])
    wait_bytes(r4.at[:, 0:1792], send4)


def sum_partials(p):
    vmem = pl.BlockSpec(memory_space=pltpu.VMEM)
    dma = pltpu.SemaphoreType.DMA
    return pl.pallas_call(
        sum_kernel,
        out_shape=jax.ShapeDtypeStruct((12, 2048), BF),
        in_specs=[vmem],
        out_specs=vmem,
        scratch_shapes=[
            pltpu.VMEM((NZ, BLOCK, 1024), BF),
            pltpu.VMEM((NZ, NX, BLOCK, 256), BF),
            pltpu.VMEM((NZ, NX, BLOCK, 256), BF),
            pltpu.VMEM((NZ, BLOCK, 256), BF),
            pltpu.VMEM((NZ, BLOCK, 256), BF),
            pltpu.VMEM((128, 256), BF),
            pltpu.VMEM((16, 2048), BF),
            dma((NZ,)), dma((NZ,)),
            dma((NZ,)), dma((NZ,)),
            dma((NZ,)), dma,
            dma, dma,
        ],
        compiler_params=pltpu.CompilerParams(
            collective_id=1, has_side_effects=True, vmem_limit_bytes=40 * 1024 * 1024
        ),
        name="sum_partials",
    )(p)


def local(tokens, norm_gain, gate_weight, up_weight, down_weight, expert_ids, expert_mix):
    gain = jnp.broadcast_to(norm_gain[:, None], (32, 128))
    gate_t, up_t, down_t = move_weights(gate_weight, up_weight, down_weight, gain)
    width = tokens.shape[2]
    token_rows = tokens.reshape(-1, width).astype(F32)
    row_mean = jnp.mean(token_rows, axis=1, keepdims=True)
    centered = token_rows - row_mean
    variance = jnp.mean(centered * centered, axis=1, keepdims=True)
    normed = (centered * lax.rsqrt(variance + norm_eps)).astype(BF)
    route_ids = expert_ids.reshape(-1, 2)
    route_mix = expert_mix.reshape(-1, 2)
    expert_iota = jnp.arange(8, dtype=jnp.int32)
    expert_gates = jnp.sum(
        (route_ids[:, :, None] == expert_iota[None, None, :]).astype(F32) * route_mix[:, :, None], axis=1
    )
    flat = (512, width)
    contract = (((1,), (1,)), ((), ()))
    gate_act = lax.dot_general(normed, gate_t.reshape(flat), contract, preferred_element_type=F32)
    up_act = lax.dot_general(normed, up_t.reshape(flat), contract, preferred_element_type=F32)
    hidden = (jax.nn.silu(gate_act) * up_act * jnp.repeat(expert_gates, 64, axis=1)).astype(BF)
    partial = jnp.dot(hidden, down_t.reshape(flat), preferred_element_type=F32).astype(BF)
    mixed = sum_partials(partial).reshape(-1, 1, width)
    turned = tuple(jnp.swapaxes(t, 1, 2) for t in (gate_t, up_t, down_t))
    return turned + (mixed,)


def solution(mesh):
    finer = Mesh(mesh.devices.reshape(NZ, NX, NC, NY), ("fs_0", "fs_1", "fs_2", "tp"))
    placed = (
        P(None, "tp", None),
        P(FS),
        P(None, FS, "tp"),
        P(None, FS, "tp"),
        P(None, FS, "tp"),
        P(None, "tp", None),
        P(None, "tp", None),
    )
    return jax.shard_map(
        local,
        mesh=finer,
        in_specs=placed,
        out_specs=(P(None, None, FS), P(None, None, FS), P(None, None, FS), P(FS, "tp", None)),
        check_vma=False,
    )
```

time: 327 us -> 160 us (0.49)
  waiting for transfers between devices: 162 us -> 0 us
  Pallas kernels: 0 us -> 129 us
  blocking collectives: 83.3 us -> 0 us
  local copies, waits for them, and re-layouts: 49.5 us -> 15.5 us
  between operations: 14.6 us -> 0.79 us
    pallas_call x0 -> x2, Pallas kernels: none -> 129 us  [the longest x1 92 us: move_weights(): pl.pallas_call(weights_kernel, out_shape=(out, out, out), in_specs=[vmem]...]
    reduce_scatter x2 -> x0, waiting for transfers between devices: 100 us -> none  [summed_rows(): so_far = lax.psum_scatter(so_far, axis, scatter_dimension=0, tiled=True)]
    all_to_all x2 -> x0, blocking collectives: 76.8 us -> none  [sent_together(): lax.all_to_all(both, axis, split_axis=split_dim, concat_axis=concat_dim,...]
    all_gather x1 -> x0, waiting for transfers between devices: 61.6 us -> none  [sent_together_2(): lax.all_gather(both, axis, axis=dim, tiled=True)]
    concatenate x2 -> x0, local copies, waits for them, and re-layouts: 11.8 us -> none  [the longest x1 7.33 us: sent_together(): both = jnp.concatenate(arrays, axis=along)]
    all_to_all x3 -> x0, local copies, waits for them, and re-layouts: 11 us -> none  [sent_together(): lax.all_to_all(both, axis, split_axis=split_dim, concat_axis=concat_dim,...]
    unnamed x21 -> x32, local copies, waits for them, and re-layouts: 19.3 us -> 10.9 us
    unnamed x1 -> x0, blocking collectives: 6.48 us -> none
  transfers between devices with their start and end apart: 4 -> 0, of which waited for: 4 -> 0; matrix products, arithmetic and copies ran while one was open for 1% -> 0% of each run, Pallas kernels for 0% -> 0%
where the time goes in v1:
time: 160 us
  Pallas kernels  129 us (81%)
  local copies, waits for them, and re-layouts  15.5 us (10%)
  matrix products  10.6 us (7%)
  other arithmetic  3.49 us (2%)
    pallas_call x1, Pallas kernels, move_weights(): pl.pallas_call(weights_kernel, out_shape=(out, out, out), in_specs=[vmem]...  92 us
    pallas_call x1, Pallas kernels, sum_partials(): pl.pallas_call(sum_kernel, out_shape=jax.ShapeDtypeStruct((12, 2048), BF)...  37.2 us
    unnamed x32, local copies, waits for them, and re-layouts  10.9 us
    dot_general x1, matrix products, local(): jnp.dot(hidden, down_t.reshape(flat), preferred_element_type=F32).astype(BF)  7.63 us
    reshape x1, local copies, waits for them, and re-layouts, local(): jnp.repeat(expert_gates, 64, axis=1)  3.24 us

profile of v1, /device:TPU:1, one launch (start us, length us, event | category | flops | bytes accessed | tf_op | source)
XLA Modules:
  0.0 159.7 jit_solution(17088350085032509623)
XLA Ops:
  0.6 0.0 copy-start.9
  0.6 2.5 %convert_reduce_fusion = f32[768]{0:T(1024)S(1)} fusion(bf16[768,1,2048]{2,0,1:T(8,128)(2,1)} %param.7), kind=kLoop, calls=%fused_computation.2 | loop fusion | flops 3144960 | bytes 3148800 | tf_op jit(solution)/shard_map/reduce_sum | solution.py:297
  3.2 0.0 copy-start.13
  3.2 0.0 copy-start.11
  3.2 0.3 copy-done.9
  3.5 1.0 fusion.4
  4.4 0.1 broadcast_in_dim.4.gain
  4.6 0.0 copy-start.8
  4.6 1.3 broadcast_in_dim.5
  5.8 3.2 %copy.16 = f32[768,512]{1,0:T(8,128)} copy(f32[768,512]{0,1:T(8,128)} %bitcast.33) | data formatting | bytes 3145728 | tf_op jit(solution)/shard_map/reshape | solution.py:311
  9.1 0.0 copy-start.10
  9.1 92.0 %move_weights.1 = (bf16[8,64,2048]{2,1,0:T(8,128)(2,1)S(1)}, bf16[8,64,2048]{2,1,0:T(8,128)(2,1)S(1)}, bf16[8,64,2048]{2,1,0:T(8,128)(2,1)S(1)}) custom-call(f32[8,32,1024]{2,1,0:T(8,128)S(1)} %copy-done.6, f32[8,32,1024]{2,1,0:T(8,128)S(1)} %copy-done.7, f32[8,32,1024]{2,1,0:T(8,128)S(1)} %copy-done.8, f32[32,128]{1,0:T(8,128)S(1)} %broadcast_in_dim.4.gain), custom_call_target="tpu_custom_call" | custom-call | tf_op jit(solution)/shard_map/move_weights/pallas_call | solution.py:160
  101.1 1.3 copy-done
  102.5 1.3 copy-done.2
  103.8 1.3 copy-done.4
  105.1 3.0 %fusion.9 = f32[768,512]{1,0:T(8,128)} fusion(bf16[512,2048]{1,0:T(8,128)(2,1)S(1)} %bitcast.30, bf16[768,1,2048]{2,0,1:T(8,128)(2,1)S(1)} %copy-done.10, f32[768]{0:T(1024)S(1)} %add_rsqrt_fusion, f32[768]{0:T(1024)S(1)} %broadcast_multiply_fusion), kind=kOutput, calls=%fused_computation.16 | convolution fusion | flops 1616904192 | bytes 6821888 | tf_op jit(solution)/shard_map/dot_general | solution.py:309
  108.1 7.6 %convolution_convert_fusion.p = bf16[768,2048]{1,0:T(8,128)(2,1)S(1)} fusion(bf16[512,2048]{1,0:T(8,128)(2,1)} %bitcast.26, f32[768,512]{1,0:T(8,128)} %copy.16, f32[768,512]{1,0:T(8,128)} %fusion.9, bf16[512,2048]{1,0:T(8,128)(2,1)} %bitcast.28, bf16[768,1,2048]{2,0,1:T(8,128)(2,1)} %param.7, f32[768]{0:T(1024)S(1)} %add_rsqrt_fusion, ...), kind=kOutput, calls=%fused_computation.8 | convolution fusion | flops 3231842304 | bytes 13637632 | tf_op jit(solution)/shard_map/dot_general | solution.py:312
  115.8 37.2 %sum_partials.1 = bf16[12,2048]{1,0:T(8,128)(2,1)S(1)} custom-call(bf16[768,2048]{1,0:T(8,128)(2,1)S(1)} %convolution_convert_fusion.p), custom_call_target="tpu_custom_call" | custom-call | tf_op jit(solution)/shard_map/sum_partials/pallas_call | solution.py:267
  153.0 1.3 copy.21
  154.4 1.0 copy-done.3
  155.4 1.3 copy.22
  156.7 1.0 copy-done.1
  157.7 1.3 copy.23
  159.0 0.6 copy.24
  (20 shorter events, 0.1 us)
Async XLA Ops:
  0.6 2.8 %copy-start.9 = (bf16[768,1,2048]{2,0,1:T(8,128)(2,1)S(1)}, bf16[768,1,2048]{2,0,1:T(8,128)(2,1)}, u32[]{:S(2)}) copy-start(bf16[768,1,2048]{2,0,1:T(8,128)(2,1)} %param.7) | copy-start | bytes 9437188
  3.2 1.3 copy-start.13
  3.2 1.3 copy-start.11
  3.2 1.3 copy-start.12
  4.5 4.5 %copy-start.6 = (f32[8,32,1024]{2,1,0:T(8,128)S(1)}, f32[8,32,1024]{2,1,0:T(8,128)}, u32[]{:S(2)}) copy-start(f32[8,32,1024]{2,1,0:T(8,128)} %gate.1) | copy-start | bytes 3145732
  4.5 4.5 %copy-start.7 = (f32[8,32,1024]{2,1,0:T(8,128)S(1)}, f32[8,32,1024]{2,1,0:T(8,128)}, u32[]{:S(2)}) copy-start(f32[8,32,1024]{2,1,0:T(8,128)} %up.1) | copy-start | bytes 3145732
  4.6 4.5 %copy-start.8 = (f32[8,32,1024]{2,1,0:T(8,128)S(1)}, f32[8,32,1024]{2,1,0:T(8,128)}, u32[]{:S(2)}) copy-start(f32[8,32,1024]{2,1,0:T(8,128)} %down.1) | copy-start | bytes 3145732
  9.1 96.0 %copy-start.10 = (bf16[768,1,2048]{2,0,1:T(8,128)(2,1)S(1)}, bf16[768,1,2048]{2,0,1:T(8,128)(2,1)}, u32[]{:S(2)}) copy-start(bf16[768,1,2048]{2,0,1:T(8,128)(2,1)} %param.7) | copy-start | bytes 9437188
  101.1 1.4 copy-start
  102.5 1.3 copy-start.2
  103.8 1.3 copy-start.4
  115.8 37.3 %copy-start.5 = (bf16[8,64,2048]{2,1,0:T(8,128)(2,1)S(1)}, bf16[8,64,2048]{2,1,0:T(8,128)(2,1)}, u32[]{:S(2)}) copy-start(bf16[8,64,2048]{2,1,0:T(8,128)(2,1)} %copy-done.4) | copy-start | bytes 6291460
  153.0 2.4 %copy-start.3 = (bf16[8,64,2048]{2,1,0:T(8,128)(2,1)S(1)}, bf16[8,64,2048]{2,1,0:T(8,128)(2,1)}, u32[]{:S(2)}) copy-start(bf16[8,64,2048]{2,1,0:T(8,128)(2,1)} %copy-done.2) | copy-start | bytes 6291460
  155.4 2.3 %copy-start.1 = (bf16[8,64,2048]{2,1,0:T(8,128)(2,1)S(1)}, bf16[8,64,2048]{2,1,0:T(8,128)(2,1)}, u32[]{:S(2)}) copy-start(bf16[8,64,2048]{2,1,0:T(8,128)(2,1)} %copy-done) | copy-start | bytes 6291460

commit v2 on v0

v2 whole, which is shorter than its diff:
```python
import jax
import jax.numpy as jnp
from jax import lax
from jax.experimental import pallas as pl
from jax.experimental.pallas import tpu as pltpu
from jax.sharding import Mesh
from jax.sharding import PartitionSpec as P

FS = ("fs_0", "fs_1", "fs_2")
NZ, NX, NC, NY = 8, 4, 2, 4
norm_eps = 1e-05
BF, F32 = jnp.bfloat16, jnp.float32
MESH = pl.DeviceIdType.MESH

CHUNKS = ((0, 0), (1, 0), (0, 1), (1, 1), (2, 0), (2, 1))
NQ = len(CHUNKS)
ROWS, WIDTH, TILE = 768, 2048, 256
BLOCK = ROWS // NZ
PIECES = 4
PIECE = WIDTH // PIECES
PASSES = 2
LANES = WIDTH // PASSES
BY_CORE = LANES // NC
BY_X = BY_CORE // NX
PAIRS = (2, 1, 3, 0)
NP = len(PAIRS)
ORDER = (
    "A0 A1 R0 A2", "R1 A3 X0 R2", "A4 X1 R3 A5", "X2 Z0 R4 X3",
    "Z1 R5 X4 X5", "Z2 N0 S0", "N1 N2 N3 N4", "Z3 N5 N6 N7", "N8 Z4 S1 F0",
    "N9 N10 N11 Z5", "S2 F1 P0", "S3 F2 P1", "H0,0 H0,1 H0,2",
    "T0 T1 F3 P2", "U0 U1 T2 T3", "P3 H1,0 H1,1 H1,2", "V0 V1 B0,0 B0,1",
    "U2 C0,0 B0,2 C0,1", "B0,3 C0,2 C0,3 U3", "D0,0 D0,1 V2 V3",
    "B1,0 E0,0 B1,1 D0,2", "E0,1 B1,2 C1,0 D0,3", "B1,3 C1,1 E0,2 C1,2",
    "C1,3 E0,3 D1,0 D1,1", "G0 E1,0 D1,2 E1,1", "D1,3 E1,2 E1,3 G1",
)


def send(src, dst, send_sem, recv_sem, to):
    pltpu.make_async_remote_copy(
        src_ref=src, dst_ref=dst, send_sem=send_sem, recv_sem=recv_sem, device_id=to, device_id_type=MESH
    ).start()


def wait_bytes(ref, sem):
    pltpu.make_async_copy(ref, ref, sem).wait()


def kernel(
    tokens, ids, mix, gain, gate, up, down,
    og, ou, od, out,
    mat, tok, xs, ar, fw, xr, ts, w, xn, gates, h,
    pb, own, r1, s1, t2, u2, r2, s2, r3, s4, r4,
    in_sem, a_send, a_recv, f_send, f_recv, x_send, x_recv, z_send, z_recv,
    c_send, c_recv, g_send, g_recv, o_sem,
    send1, recv1, send2, recv2, sendt, recvt, send3, recv3, send4, recv4,
):
    z, x, c, y = (lax.axis_index(a) for a in ("fs_0", "fs_1", "fs_2", "tp"))
    me = 2 * x + c
    ahead, behind, across = (lax.rem(y + o, NY) for o in (1, 3, 2))
    right, left, opposite = (lax.rem(x + o, NX) for o in (1, 3, 2))
    column = pl.multiple_of(256 * z, 256)

    reads = [pltpu.make_async_copy(r, mat.at[m], in_sem.at[m]) for m, r in enumerate((gate, up, down))]
    reads.append(pltpu.make_async_copy(tokens, tok, in_sem.at[3]))
    for r in reads:
        r.start()

    barrier = pltpu.get_barrier_semaphore()
    peers = []
    for off in range(1, NX * NC):
        j = lax.rem(me + off, NX * NC)
        peers.append({"fs_1": j // 2, "fs_2": lax.rem(j, 2)})
    for off in range(1, NZ):
        peers.append({"fs_0": lax.rem(z + off, NZ)})
    peers += [{"tp": ahead}, {"tp": behind}]
    for to in peers:
        pl.semaphore_signal(barrier, inc=1, device_id=to, device_id_type=MESH)

    def pack(q):
        m, el = CHUNKS[q]
        low = lax.broadcasted_iota(jnp.int32, (32, 128), 1) < 64
        eye = lax.broadcasted_iota(jnp.int32, (32, 32), 0) == lax.broadcasted_iota(jnp.int32, (32, 32), 1)
        scale = jnp.sum(jnp.where(eye, gain[...], 0.0), axis=1, keepdims=True)

        def one(i, carry):
            ep, xp = i // NX, lax.rem(i, NX)
            at = pl.multiple_of(128 * xp, 128)
            a = mat[m, 2 * ep + el, :, pl.ds(at, 128)]
            b = mat[m, 2 * ep + el, :, pl.ds(pl.multiple_of(512 + at, 128), 128)]
            if m < 2:
                a, b = a * scale, b * scale
            xs[q, ep, 2 * xp] = jnp.where(low, a, pltpu.roll(b, 64, 1)).astype(BF)
            xs[q, ep, 2 * xp + 1] = jnp.where(low, pltpu.roll(a, 64, 1), b).astype(BF)
            return carry

        lax.fori_loop(0, 4 * NX, one, 0, unroll=4)

    def over_planes(q):
        send(xs.at[q, across, 0:4], fw.at[q, 0], a_send.at[q], f_recv.at[q, 0], {"tp": ahead})
        send(xs.at[q, across, 4:8], fw.at[q, 1], a_send.at[q], f_recv.at[q, 1], {"tp": behind})
        send(xs.at[q, ahead], ar.at[q, y], a_send.at[q], a_recv.at[q], {"tp": ahead})
        send(xs.at[q, behind], ar.at[q, y], a_send.at[q], a_recv.at[q], {"tp": behind})
        ar[q, y] = xs[q, y]

    def relay(q):
        wait_bytes(fw.at[q, 0], f_recv.at[q, 0])
        send(fw.at[q, 0], ar.at[q, behind, 0:4], f_send.at[q], a_recv.at[q], {"tp": ahead})
        wait_bytes(fw.at[q, 1], f_recv.at[q, 1])
        send(fw.at[q, 1], ar.at[q, ahead, 4:8], f_send.at[q], a_recv.at[q], {"tp": behind})

    def over_x(q):
        wait_bytes(ar.at[q, 0:3], a_recv.at[q])
        for off in range(1, NX * NC):
            j = lax.rem(me + off, NX * NC)
            send(
                ar.at[q, :, j], xr.at[q, me], x_send.at[q], x_recv.at[q],
                {"fs_1": j // 2, "fs_2": lax.rem(j, 2)},
            )
        xr[q, me] = ar[q, :, me]

    def over_z(q):
        wait_bytes(xr.at[q, 0:7], x_recv.at[q])

        def one(y0, carry):
            for half in range(2):
                rows = jnp.concatenate([xr[q, 4 * half + k, y0] for k in range(4)], axis=0)
                ts[q, y0, :, 128 * half : 128 * (half + 1)] = rows.T
            return carry

        lax.fori_loop(0, NY, one, 0)
        for off in (4, 3, 5, 2, 6, 1, 7):
            zp = lax.rem(z + off, NZ)
            rows = pl.multiple_of(64 * lax.rem(zp, 2), 64)
            send(
                ts.at[q, zp // 2, pl.ds(rows, 64), :], w.at[q, y, :, pl.ds(column, 256)],
                z_send.at[q], z_recv.at[q], {"fs_0": zp},
            )
        rows = pl.multiple_of(64 * lax.rem(z, 2), 64)
        w[q, y, :, pl.ds(column, 256)] = ts[q, z // 2, pl.ds(rows, 64), :]

    def spread(q):
        wait_bytes(w.at[q, 0, :, 0:1792], z_recv.at[q])
        send(w.at[q, y], w.at[q, y], c_send.at[q], c_recv.at[q, 0], {"tp": ahead})
        send(w.at[q, y], w.at[q, y], c_send.at[q], c_recv.at[q, 1], {"tp": behind})

    def spread_on(q):
        wait_bytes(w.at[q, behind], c_recv.at[q, 0])
        send(w.at[q, behind, 0:32], w.at[q, behind, 0:32], g_send.at[q], g_recv.at[q], {"tp": ahead})
        wait_bytes(w.at[q, ahead], c_recv.at[q, 1])
        send(w.at[q, ahead, 32:64], w.at[q, ahead, 32:64], g_send.at[q], g_recv.at[q], {"tp": behind})

    def arrived(q):
        wait_bytes(w.at[q, across], g_recv.at[q])
        m, el = CHUNKS[q]
        for ep in range(NY):
            pltpu.make_async_copy(w.at[q, ep], (og, ou)[m].at[2 * ep + el], o_sem.at[q]).start()

    def piece(p, plane):
        return w.at[4:6, plane, :, PIECE * p : PIECE * (p + 1)]

    def spread_down(p):
        if p == 0:
            for q in (4, 5):
                wait_bytes(w.at[q, 0, :, 0:1792], z_recv.at[q])
        send(piece(p, y), piece(p, y), c_send.at[4 + p], c_recv.at[4 + p, 0], {"tp": ahead})
        send(piece(p, y), piece(p, y), c_send.at[4 + p], c_recv.at[4 + p, 1], {"tp": behind})

    def spread_down_on(p):
        wait_bytes(piece(p, behind), c_recv.at[4 + p, 0])
        part = piece(p, behind).at[0]
        send(part, part, g_send.at[4 + p], g_recv.at[4 + p], {"tp": ahead})
        wait_bytes(piece(p, ahead), c_recv.at[4 + p, 1])
        part = piece(p, ahead).at[1]
        send(part, part, g_send.at[4 + p], g_recv.at[4 + p], {"tp": behind})

    def arrived_down(p):
        wait_bytes(piece(p, across), g_recv.at[4 + p])
        lanes = slice(PIECE * p, PIECE * (p + 1))
        for ep in range(NY):
            for el in range(2):
                pltpu.make_async_copy(
                    w.at[4 + el, ep, :, lanes], od.at[2 * ep + el, :, lanes], o_sem.at[4 + p]
                ).start()

    def normalize(i):
        if i == 0:
            reads[3].wait()
            expert = lax.broadcasted_iota(jnp.int32, (8, ROWS), 0)
            by_expert = jnp.where(ids[0:1, :] == expert, mix[0:1, :], 0.0)
            by_expert = by_expert + jnp.where(ids[1:2, :] == expert, mix[1:2, :], 0.0)
            gates[...] = by_expert.T

        def one(j, carry):
            rows = pl.ds(pl.multiple_of(64 * i + 16 * j, 16), 16)
            v = tok[rows, :].astype(F32)
            v = v - jnp.mean(v, axis=1, keepdims=True)
            var = jnp.mean(v * v, axis=1, keepdims=True)
            xn[rows, :] = (v * lax.rsqrt(var + norm_eps)).astype(BF)
            return carry

        lax.fori_loop(0, 4, one, 0, unroll=4)

    contract = (((1,), (1,)), ((), ()))

    def hide(el, i):
        rows = pl.ds(TILE * i, TILE)
        v = xn[rows, :]
        low = lax.broadcasted_iota(jnp.int32, (TILE, 128), 1) < 64
        first = 2 * el
        for pair in range(2):
            wg = w[first, 2 * pair : 2 * pair + 2].reshape(128, WIDTH)
            wu = w[first + 1, 2 * pair : 2 * pair + 2].reshape(128, WIDTH)
            g = lax.dot_general(v, wg, contract, preferred_element_type=F32)
            u = lax.dot_general(v, wu, contract, preferred_element_type=F32)
            e = 4 * pair + el
            share = jnp.where(low, gates[rows, e : e + 1], gates[rows, e + 2 : e + 3])
            h[rows, 256 * el + 128 * pair : 256 * el + 128 * (pair + 1)] = (
                g / (1.0 + jnp.exp(-g)) * u * share
            ).astype(BF)

    def part(rows, at):
        v = h[rows, :]
        a = w[4, :, :, pl.ds(at, BY_CORE)].reshape(256, BY_CORE)
        b = w[5, :, :, pl.ds(at, BY_CORE)].reshape(256, BY_CORE)
        return jnp.dot(v[:, 0:256], a, preferred_element_type=F32) + jnp.dot(
            v[:, 256:512], b, preferred_element_type=F32
        )

    def pair_of(k):
        return lax.rem(z // 2 + PAIRS[k], NP)

    def between_cores(s, k):
        i = NP * s + k
        rows = pl.ds(pl.multiple_of(2 * BLOCK * pair_of(k), 2 * BLOCK), 2 * BLOCK)
        pb[i] = part(rows, pl.multiple_of(LANES * s + BY_CORE * (1 - c), BY_CORE)).astype(BF)
        send(pb.at[i], r1.at[i], send1.at[i], recv1.at[i], {"fs_2": 1 - c})
        own[i] = part(rows, pl.multiple_of(LANES * s + BY_CORE * c, BY_CORE))

    def sum_x(s, k):
        i = NP * s + k
        wait_bytes(r1.at[i], recv1.at[i])
        total = (own[i] + r1[i].astype(F32)).astype(BF)
        for xp in range(NX):
            for half in range(2):
                s1[i, xp, half] = total[BLOCK * half : BLOCK * (half + 1), BY_X * xp : BY_X * (xp + 1)]
        send(s1.at[i, opposite, 0], t2.at[i, 0], sendt.at[i], recvt.at[i, 0], {"fs_1": right})
        send(s1.at[i, opposite, 1], t2.at[i, 1], sendt.at[i], recvt.at[i, 1], {"fs_1": left})
        send(s1.at[i, right, 1], r2.at[i, 1, 1], send2.at[i], recv2.at[i], {"fs_1": right})
        send(s1.at[i, left, 0], r2.at[i, 0, 1], send2.at[i], recv2.at[i], {"fs_1": left})

    def sum_x_on(s, k):
        i = NP * s + k
        wait_bytes(t2.at[i, 0], recvt.at[i, 0])
        u2[i, 0] = (s1[i, right, 0].astype(F32) + t2[i, 0].astype(F32)).astype(BF)
        send(u2.at[i, 0], r2.at[i, 0, 0], send2.at[i], recv2.at[i], {"fs_1": right})
        wait_bytes(t2.at[i, 1], recvt.at[i, 1])
        u2[i, 1] = (s1[i, left, 1].astype(F32) + t2[i, 1].astype(F32)).astype(BF)
        send(u2.at[i, 1], r2.at[i, 1, 0], send2.at[i], recv2.at[i], {"fs_1": left})

    def sum_z(s, k):
        i = NP * s + k
        wait_bytes(r2.at[i], recv2.at[i])
        for half in range(2):
            total = s1[i, x, half].astype(F32) + (r2[i, half, 0].astype(F32) + r2[i, half, 1].astype(F32))
            s2[i, half] = total.astype(BF)
        if PAIRS[k] == 0:
            here = lax.rem(z, 2)
            send(s2.at[i, 1 - here], r3.at[s, z], send3.at[i], recv3.at[s], {"fs_0": z + 1 - 2 * here})
            r3[s, z] = s2[i, here]
        else:
            for half in range(2):
                send(s2.at[i, half], r3.at[s, z], send3.at[i], recv3.at[s], {"fs_0": 2 * pair_of(k) + half})

    def give_rows(s):
        wait_bytes(r3.at[s, 0:7], recv3.at[s])
        total = r3[s, 0].astype(F32)
        for i in range(1, NZ):
            total = total + r3[s, i].astype(F32)
        row = lax.broadcasted_iota(jnp.int32, (128, BLOCK), 0)
        col = lax.broadcasted_iota(jnp.int32, (128, BLOCK), 1)
        within = lax.rem(row, 16)
        pick = ((col == (row // 16) * 12 + within) & (within < 12)).astype(BF)
        s4[s] = jnp.dot(pick, total.astype(BF), preferred_element_type=F32).astype(BF)
        at = pl.multiple_of(LANES * s + BY_CORE * c + BY_X * x, BY_X)
        for off in range(1, NX * NC):
            j = lax.rem(me + off, NX * NC)
            send(
                s4.at[s, pl.ds(pl.multiple_of(16 * j, 16), 16), :], r4.at[:, pl.ds(at, BY_X)],
                send4.at[s], recv4.at[s], {"fs_1": j // 2, "fs_2": lax.rem(j, 2)},
            )
        r4[:, pl.ds(at, BY_X)] = s4[s, pl.ds(pl.multiple_of(16 * me, 16), 16), :]

    for q in range(NQ):
        m, el = CHUNKS[q]
        if q in (0, 1, 4):
            reads[m].wait()
        pack(q)
    pl.semaphore_wait(barrier, len(peers))
    names = dict(
        A=over_planes, R=relay, X=over_x, Z=over_z, S=spread, F=spread_on, P=arrived, N=normalize, H=hide,
        T=spread_down, U=spread_down_on, V=arrived_down,
        B=between_cores, C=sum_x, D=sum_x_on, E=sum_z, G=give_rows,
    )
    for line in ORDER:
        for step in line.split():
            name, args = step[0], step[1:].split(",")
            names[name](*(int(a) for a in args))

    for q in range(NQ):
        wait_bytes(ar.at[q, 0:3], a_send.at[q])
        wait_bytes(fw.at[q], f_send.at[q])
        wait_bytes(xr.at[q, 0:7], x_send.at[q])
        wait_bytes(w.at[q, 0, :, 0:1792], z_send.at[q])
    for q in range(4):
        wait_bytes(w.at[q, 0:2], c_send.at[q])
        wait_bytes(w.at[q, 0], g_send.at[q])
        wait_bytes(w.at[q], o_sem.at[q])
    for p in range(PIECES):
        wait_bytes(w.at[4, :, :, 0:PIECE], c_send.at[4 + p])
        wait_bytes(piece(p, 0), g_send.at[4 + p])
        wait_bytes(w.at[4:6, :, :, 0:PIECE], o_sem.at[4 + p])
    for s in range(PASSES):
        for k in range(NP):
            i = NP * s + k
            wait_bytes(pb.at[i], send1.at[i])
            wait_bytes(t2.at[i], sendt.at[i])
            wait_bytes(r2.at[i], send2.at[i])
            if PAIRS[k] == 0:
                wait_bytes(s2.at[i, 0], send3.at[i])
            else:
                wait_bytes(s2.at[i], send3.at[i])
        wait_bytes(r4.at[:, 0 : 7 * BY_X], recv4.at[s])
    out[...] = r4[0:12, :]
    for s in range(PASSES):
        wait_bytes(r4.at[:, 0 : 7 * BY_X], send4.at[s])


def run(*args):
    weights = jax.ShapeDtypeStruct((8, 64, WIDTH), BF)
    vmem = pl.BlockSpec(memory_space=pltpu.VMEM)
    hbm = pl.BlockSpec(memory_space=pl.ANY)
    dma = pltpu.SemaphoreType.DMA
    return pl.pallas_call(
        kernel,
        out_shape=(weights, weights, weights, jax.ShapeDtypeStruct((12, WIDTH), BF)),
        in_specs=[hbm, vmem, vmem, vmem, hbm, hbm, hbm],
        out_specs=(hbm, hbm, hbm, vmem),
        scratch_shapes=[
            pltpu.VMEM((3, 8, 32, 1024), F32),
            pltpu.VMEM((ROWS, WIDTH), BF),
            pltpu.VMEM((NQ, NY, 8, 32, 128), BF),
            pltpu.VMEM((NQ, NY, 8, 32, 128), BF),
            pltpu.VMEM((NQ, 2, 4, 32, 128), BF),
            pltpu.VMEM((NQ, 8, NY, 32, 128), BF),
            pltpu.VMEM((NQ, NY, 128, 256), BF),
            pltpu.VMEM((NQ, NY, 64, WIDTH), BF),
            pltpu.VMEM((ROWS, WIDTH), BF),
            pltpu.VMEM((ROWS, 8), F32),
            pltpu.VMEM((ROWS, 512), BF),
            pltpu.VMEM((PASSES * NP, 2 * BLOCK, BY_CORE), BF),
            pltpu.VMEM((PASSES * NP, 2 * BLOCK, BY_CORE), F32),
            pltpu.VMEM((PASSES * NP, 2 * BLOCK, BY_CORE), BF),
            pltpu.VMEM((PASSES * NP, NX, 2, BLOCK, BY_X), BF),
            pltpu.VMEM((PASSES * NP, 2, BLOCK, BY_X), BF),
            pltpu.VMEM((PASSES * NP, 2, BLOCK, BY_X), BF),
            pltpu.VMEM((PASSES * NP, 2, 2, BLOCK, BY_X), BF),
            pltpu.VMEM((PASSES * NP, 2, BLOCK, BY_X), BF),
            pltpu.VMEM((PASSES, NZ, BLOCK, BY_X), BF),
            pltpu.VMEM((PASSES, 128, BY_X), BF),
            pltpu.VMEM((16, WIDTH), BF),
            dma((4,)),
            dma((NQ,)), dma((NQ,)),
            dma((NQ,)), dma((NQ, 2)),
            dma((NQ,)), dma((NQ,)),
            dma((NQ,)), dma((NQ,)),
            dma((4 + PIECES,)), dma((4 + PIECES, 2)),
            dma((4 + PIECES,)), dma((4 + PIECES,)),
            dma((4 + PIECES,)),
            dma((PASSES * NP,)), dma((PASSES * NP,)),
            dma((PASSES * NP,)), dma((PASSES * NP,)),
            dma((PASSES * NP,)), dma((PASSES * NP, 2)),
            dma((PASSES * NP,)), dma((PASSES,)),
            dma((PASSES,)), dma((PASSES,)),
        ],
        compiler_params=pltpu.CompilerParams(
            collective_id=0, has_side_effects=True, vmem_limit_bytes=60 * 1024 * 1024
        ),
        name="hand_over_and_serve",
    )(*args)


def put_kernel(wg, wu, wd, small, og, ou, od, out, buf, buf_small, sems):
    hops = [(small, buf_small, out)]
    for m, (w, o) in enumerate(((wg, og), (wu, ou), (wd, od))):
        for i in range(4):
            two = slice(2 * i, 2 * i + 2)
            hops.append((w.at[two], buf.at[m, two], o.at[two]))
    reads = [pltpu.make_async_copy(a, b, sems.at[0, n]) for n, (a, b, _) in enumerate(hops)]
    writes = [pltpu.make_async_copy(b, o, sems.at[1, n]) for n, (_, b, o) in enumerate(hops)]
    for copy in reads:
        copy.start()
    for read, write in zip(reads, writes):
        read.wait()
        write.start()
    for copy in writes:
        copy.wait()


def put_out(*results):
    weights = jax.ShapeDtypeStruct((8, 64, WIDTH), BF)
    small = jax.ShapeDtypeStruct((12, WIDTH), BF)
    hbm = pl.BlockSpec(memory_space=pl.ANY)
    return pl.pallas_call(
        put_kernel,
        out_shape=(weights, weights, weights, small),
        in_specs=[hbm] * 4,
        out_specs=(hbm, hbm, hbm, hbm),
        scratch_shapes=[
            pltpu.VMEM((3, 8, 64, WIDTH), BF),
            pltpu.VMEM((12, WIDTH), BF),
            pltpu.SemaphoreType.DMA((2, 13)),
        ],
        compiler_params=pltpu.CompilerParams(vmem_limit_bytes=60 * 1024 * 1024),
        name="put_out",
    )(*results)


def local(tokens, norm_gain, gate_weight, up_weight, down_weight, expert_ids, expert_mix):
    results = run(
        tokens.reshape(ROWS, WIDTH), expert_ids.reshape(ROWS, 2).T, expert_mix.reshape(ROWS, 2).T,
        norm_gain.reshape(1, 32), gate_weight, up_weight, down_weight,
    )
    gate_t, up_t, down_t, mixed = put_out(*results)
    turned = tuple(jnp.swapaxes(t, 1, 2) for t in (gate_t, up_t, down_t))
    return turned + (mixed.reshape(12, 1, WIDTH),)


def solution(mesh):
    finer = Mesh(mesh.devices.reshape(NZ, NX, NC, NY), ("fs_0", "fs_1", "fs_2", "tp"))
    placed = (
        P(None, "tp", None),
        P(FS),
        P(None, FS, "tp"),
        P(None, FS, "tp"),
        P(None, FS, "tp"),
        P(None, "tp", None),
        P(None, "tp", None),
    )
    return jax.shard_map(
        local,
        mesh=finer,
        in_specs=placed,
        out_specs=(P(None, None, FS), P(None, None, FS), P(None, None, FS), P(FS, "tp", None)),
        check_vma=False,
    )
```

time: 327 us -> 120 us (0.37)
  waiting for transfers between devices: 162 us -> 0 us
  Pallas kernels: 0 us -> 119 us
  blocking collectives: 83.3 us -> 0 us
  local copies, waits for them, and re-layouts: 49.5 us -> 0 us
  between operations: 14.6 us -> 0.8 us
  matrix products: 8.38 us -> 0 us
  other arithmetic: 6.63 us -> 0 us
    pallas_call x0 -> x2, Pallas kernels: none -> 119 us  [the longest x1 113 us: run(): pl.pallas_call(kernel, out_shape=(weights, weights, weights, jax.ShapeDty...]
    reduce_scatter x2 -> x0, waiting for transfers between devices: 100 us -> none  [summed_rows(): so_far = lax.psum_scatter(so_far, axis, scatter_dimension=0, tiled=True)]
    all_to_all x2 -> x0, blocking collectives: 76.8 us -> none  [sent_together(): lax.all_to_all(both, axis, split_axis=split_dim, concat_axis=concat_dim,...]
    all_gather x1 -> x0, waiting for transfers between devices: 61.6 us -> none  [sent_together_2(): lax.all_gather(both, axis, axis=dim, tiled=True)]
    unnamed x21 -> x0, local copies, waits for them, and re-layouts: 19.3 us -> none
    concatenate x2 -> x0, local copies, waits for them, and re-layouts: 11.8 us -> none  [the longest x1 7.33 us: sent_together(): both = jnp.concatenate(arrays, axis=along)]
    all_to_all x3 -> x0, local copies, waits for them, and re-layouts: 11 us -> none  [sent_together(): lax.all_to_all(both, axis, split_axis=split_dim, concat_axis=concat_dim,...]
    unnamed x1 -> x0, blocking collectives: 6.48 us -> none
  transfers between devices with their start and end apart: 4 -> 0, of which waited for: 4 -> 0; matrix products, arithmetic and copies ran while one was open for 1% -> 0% of each run, Pallas kernels for 0% -> 0%
where the time goes in v2:
time: 120 us; the launch traced here: 119 us
  Pallas kernels  119 us (99%)
    pallas_call x1, Pallas kernels, run(): pl.pallas_call(kernel, out_shape=(weights, weights, weights, jax.ShapeDty...  113 us
    pallas_call x1, Pallas kernels, put_out(): pl.pallas_call(put_kernel, out_shape=(weights, weights, weights, small),...  5.54 us

profile of v2, /device:TPU:1, one launch (start us, length us, event | category | flops | bytes accessed | tf_op | source)
XLA Modules:
  0.0 119.4 jit_solution(11867635555088718930)
XLA Ops:
  0.6 113.1 %hand_over_and_serve.1 = (bf16[8,64,2048]{2,1,0:T(8,128)(2,1)}, bf16[8,64,2048]{2,1,0:T(8,128)(2,1)}, bf16[8,64,2048]{2,1,0:T(8,128)(2,1)}, bf16[12,2048]{1,0:T(8,128)(2,1)}) custom-call(bf16[768,2048]{1,0:T(8,128)(2,1)} %bitcast.12, s32[2,768]{1,0:T(2,128)} %bitcast.13, f32[2,768]{1,0:T(2,128)} %bitcast.14, f32[1,32]{1,0:T(1,128)} %bitcast.15, ...), custom_call_target="tpu_custom_call" | custom-call | tf_op jit(solution)/shard_map/hand_over_and_serve/pallas_call | solution.py:343
  113.7 5.5 %put_out.1 = (bf16[8,64,2048]{2,1,0:T(8,128)(2,1)}, bf16[8,64,2048]{2,1,0:T(8,128)(2,1)}, bf16[8,64,2048]{2,1,0:T(8,128)(2,1)}, bf16[12,2048]{1,0:T(8,128)(2,1)}) custom-call(bf16[8,64,2048]{2,1,0:T(8,128)(2,1)} %get-tuple-element.12.wg, bf16[8,64,2048]{2,1,0:T(8,128)(2,1)} %get-tuple-element.13.wu, bf16[8,64,2048]{2,1,0:T(8,128)(2,1)} %get-tuple-element.14.wd, ...), custom_call_target="tpu_custom_call" | custom-call | tf_op jit(solution)/shard_map/put_out/pallas_call | solution.py:413

commit v3 on v2

--- a/solution.py
+++ b/solution.py
@@ -14,24 +14,25 @@
 
 CHUNKS = ((0, 0), (1, 0), (0, 1), (1, 1), (2, 0), (2, 1))
 NQ = len(CHUNKS)
-ROWS, WIDTH, TILE = 768, 2048, 256
+ROWS, WIDTH = 768, 2048
 BLOCK = ROWS // NZ
-PIECES = 4
-PIECE = WIDTH // PIECES
-PASSES = 2
-LANES = WIDTH // PASSES
-BY_CORE = LANES // NC
-BY_X = BY_CORE // NX
-PAIRS = (2, 1, 3, 0)
-NP = len(PAIRS)
+EARLY = 2
+PASSES = 4
+PIECE = WIDTH // PASSES
+BY_X = PIECE // NX
+NP = 2
+PART = ROWS // NC // NP
+SHARE = BLOCK // NC
 ORDER = (
-    "A0 A1 R0 A2", "R1 A3 X0 R2", "A4 X1 R3 A5", "X2 Z0 R4 X3",
-    "Z1 R5 X4 X5", "Z2 N0 S0", "N1 N2 N3 N4", "Z3 N5 N6 N7", "N8 Z4 S1 F0",
-    "N9 N10 N11 Z5", "S2 F1 P0", "S3 F2 P1", "H0,0 H0,1 H0,2",
-    "T0 T1 F3 P2", "U0 U1 T2 T3", "P3 H1,0 H1,1 H1,2", "V0 V1 B0,0 B0,1",
-    "U2 C0,0 B0,2 C0,1", "B0,3 C0,2 C0,3 U3", "D0,0 D0,1 V2 V3",
-    "B1,0 E0,0 B1,1 D0,2", "E0,1 B1,2 C1,0 D0,3", "B1,3 C1,1 E0,2 C1,2",
-    "C1,3 E0,3 D1,0 D1,1", "G0 E1,0 D1,2 E1,1", "D1,3 E1,2 E1,3 G1",
+    "A0 K1 A1 K2", "K3 K4 K5 R0", "A2 X0 R1 A3", "R2", "X1 A4 R3 X2", "Z0 A5 Q0,0 R4",
+    "X3 Q0,1 Q0,7 Z1", "R5 Q1,0 X4 Q0,2", "Q0,6 X5 Z2 Q1,1", "Q1,7 Q0,3 Q0,5 N0",
+    "Z3 Q1,2 Q1,6 N1", "Q0,4 Z4 N2 N3", "Q1,3 Q1,5 F0", "Z5 N4 N5",
+    "Q1,4 N6 N7", "S2 N8 F1", "N9 N10 N11 P0",
+    "S3 F2 P1", "H0,0 H0,1", "F3 T0 T1 P2", "P3 H1,0 H1,1",
+    "U0 T2 U1 T3", "V0 B0,0 B0,1 U2", "C0,0 C0,1 V1 B1,0",
+    "B1,1 U3 D0,0 C1,0", "D0,1 C1,1 V2", "B2,0 B2,1 E0,0 V3",
+    "B3,0 B3,1 D1,0 E0,1", "C2,0 D1,1 C2,1 C3,0", "C3,1 E1,0 D2,0 G0",
+    "E1,1 D2,1 D3,0 D3,1", "E2,0 G1 E2,1 E3,0", "E3,1 G2 G3",
 )
 
 
@@ -46,11 +47,11 @@
 
 
 def kernel(
-    tokens, ids, mix, gain, gate, up, down,
+    tokens, ids_in, mix_in, gain_in, gate, up, down,
     og, ou, od, out,
-    mat, tok, xs, ar, fw, xr, ts, w, xn, gates, h,
+    ids, mix, gain, mat, tok, xs, ar, fw, xr, ts, w, xn, gates, h,
     pb, own, r1, s1, t2, u2, r2, s2, r3, s4, r4,
-    in_sem, a_send, a_recv, f_send, f_recv, x_send, x_recv, z_send, z_recv,
+    in_sem, a_send, a_recv, f_send, f_recv, x_send, x_recv, z_send, z_recv, n_recv,
     c_send, c_recv, g_send, g_recv, o_sem,
     send1, recv1, send2, recv2, sendt, recvt, send3, recv3, send4, recv4,
 ):
@@ -60,8 +61,8 @@
     right, left, opposite = (lax.rem(x + o, NX) for o in (1, 3, 2))
     column = pl.multiple_of(256 * z, 256)
 
-    reads = [pltpu.make_async_copy(r, mat.at[m], in_sem.at[m]) for m, r in enumerate((gate, up, down))]
-    reads.append(pltpu.make_async_copy(tokens, tok, in_sem.at[3]))
+    pairs = ((gain_in, gain), (gate, mat.at[0]), (up, mat.at[1]), (down, mat.at[2]), (tokens, tok), (ids_in, ids), (mix_in, mix))
+    reads = [pltpu.make_async_copy(src, dst, in_sem.at[n]) for n, (src, dst) in enumerate(pairs)]
     for r in reads:
         r.start()
 
@@ -78,6 +79,10 @@
 
     def pack(q):
         m, el = CHUNKS[q]
+        if q == 0:
+            reads[0].wait()
+        if el == 0:
+            reads[1 + m].wait()
         low = lax.broadcasted_iota(jnp.int32, (32, 128), 1) < 64
         eye = lax.broadcasted_iota(jnp.int32, (32, 32), 0) == lax.broadcasted_iota(jnp.int32, (32, 32), 1)
         scale = jnp.sum(jnp.where(eye, gain[...], 0.0), axis=1, keepdims=True)
@@ -128,15 +133,23 @@
             return carry
 
         lax.fori_loop(0, NY, one, 0)
-        for off in (4, 3, 5, 2, 6, 1, 7):
+        for off in (1, 7, 2, 6, 3, 5, 4) if q < EARLY else (4, 3, 5, 2, 6, 1, 7):
             zp = lax.rem(z + off, NZ)
             rows = pl.multiple_of(64 * lax.rem(zp, 2), 64)
             send(
                 ts.at[q, zp // 2, pl.ds(rows, 64), :], w.at[q, y, :, pl.ds(column, 256)],
-                z_send.at[q], z_recv.at[q], {"fs_0": zp},
+                z_send.at[q], n_recv.at[q, off] if q < EARLY else z_recv.at[q], {"fs_0": zp},
             )
         rows = pl.multiple_of(64 * lax.rem(z, 2), 64)
         w[q, y, :, pl.ds(column, 256)] = ts[q, z // 2, pl.ds(rows, 64), :]
+
+    def spread_first(q, off):
+        lanes = pl.ds(pl.multiple_of(256 * lax.rem(z + NZ - off, NZ), 256), 256)
+        if off > 0:
+            wait_bytes(w.at[q, 0, :, 0:256], n_recv.at[q, off])
+        block = w.at[q, y, :, lanes]
+        send(block, block, c_send.at[q], c_recv.at[q, 0], {"tp": ahead})
+        send(block, block, c_send.at[q], c_recv.at[q, 1], {"tp": behind})
 
     def spread(q):
         wait_bytes(w.at[q, 0, :, 0:1792], z_recv.at[q])
@@ -184,7 +197,8 @@
 
     def normalize(i):
         if i == 0:
-            reads[3].wait()
+            for r in reads[4:]:
+                r.wait()
             expert = lax.broadcasted_iota(jnp.int32, (8, ROWS), 0)
             by_expert = jnp.where(ids[0:1, :] == expert, mix[0:1, :], 0.0)
             by_expert = by_expert + jnp.where(ids[1:2, :] == expert, mix[1:2, :], 0.0)
@@ -203,9 +217,9 @@
     contract = (((1,), (1,)), ((), ()))
 
     def hide(el, i):
-        rows = pl.ds(TILE * i, TILE)
+        rows = pl.ds(NC * PART * i, NC * PART)
         v = xn[rows, :]
-        low = lax.broadcasted_iota(jnp.int32, (TILE, 128), 1) < 64
+        low = lax.broadcasted_iota(jnp.int32, (NC * PART, 128), 1) < 64
         first = 2 * el
         for pair in range(2):
             wg = w[first, 2 * pair : 2 * pair + 2].reshape(128, WIDTH)
@@ -214,27 +228,31 @@
             u = lax.dot_general(v, wu, contract, preferred_element_type=F32)
             e = 4 * pair + el
             share = jnp.where(low, gates[rows, e : e + 1], gates[rows, e + 2 : e + 3])
-            h[rows, 256 * el + 128 * pair : 256 * el + 128 * (pair + 1)] = (
-                g / (1.0 + jnp.exp(-g)) * u * share
-            ).astype(BF)
-
-    def part(rows, at):
-        v = h[rows, :]
-        a = w[4, :, :, pl.ds(at, BY_CORE)].reshape(256, BY_CORE)
-        b = w[5, :, :, pl.ds(at, BY_CORE)].reshape(256, BY_CORE)
+            hid = (g / (1.0 + jnp.exp(-g)) * u * share).astype(BF)
+            at = 256 * el + 128 * pair
+            for b in range(NZ // NP):
+                for core in range(NC):
+                    h[core, PART * i + SHARE * b : PART * i + SHARE * (b + 1), at : at + 128] = hid[
+                        BLOCK * b + SHARE * core : BLOCK * b + SHARE * (core + 1)
+                    ]
+
+    def side_of(k):
+        return lax.rem(z // 4 + 1 - k, NP)
+
+    def part(s, k, core):
+        v = h[core, pl.ds(pl.multiple_of(PART * side_of(k), PART), PART), :]
+        lanes = slice(PIECE * s, PIECE * (s + 1))
+        a = w[4, :, :, lanes].reshape(256, PIECE)
+        b = w[5, :, :, lanes].reshape(256, PIECE)
         return jnp.dot(v[:, 0:256], a, preferred_element_type=F32) + jnp.dot(
             v[:, 256:512], b, preferred_element_type=F32
         )
 
-    def pair_of(k):
-        return lax.rem(z // 2 + PAIRS[k], NP)
-
     def between_cores(s, k):
         i = NP * s + k
-        rows = pl.ds(pl.multiple_of(2 * BLOCK * pair_of(k), 2 * BLOCK), 2 * BLOCK)
-        pb[i] = part(rows, pl.multiple_of(LANES * s + BY_CORE * (1 - c), BY_CORE)).astype(BF)
+        pb[i] = part(s, k, 1 - c).astype(BF)
         send(pb.at[i], r1.at[i], send1.at[i], recv1.at[i], {"fs_2": 1 - c})
-        own[i] = part(rows, pl.multiple_of(LANES * s + BY_CORE * c, BY_CORE))
+        own[i] = part(s, k, c)
 
     def sum_x(s, k):
         i = NP * s + k
@@ -262,42 +280,63 @@
         wait_bytes(r2.at[i], recv2.at[i])
         for half in range(2):
             total = s1[i, x, half].astype(F32) + (r2[i, half, 0].astype(F32) + r2[i, half, 1].astype(F32))
-            s2[i, half] = total.astype(BF)
-        if PAIRS[k] == 0:
-            here = lax.rem(z, 2)
-            send(s2.at[i, 1 - here], r3.at[s, z], send3.at[i], recv3.at[s], {"fs_0": z + 1 - 2 * here})
+            for two in range(2):
+                s2[i, 2 * half + two] = total[SHARE * two : SHARE * (two + 1)].astype(BF)
+        here = lax.rem(z, 4)
+        for step in range(k, 4):
+            b = lax.rem(here + step, 4)
+            send(s2.at[i, b], r3.at[s, z], send3.at[i], recv3.at[s], {"fs_0": 4 * side_of(k) + b})
+        if k == 1:
             r3[s, z] = s2[i, here]
-        else:
-            for half in range(2):
-                send(s2.at[i, half], r3.at[s, z], send3.at[i], recv3.at[s], {"fs_0": 2 * pair_of(k) + half})
+
+    amid = x // 2 == c
 
     def give_rows(s):
         wait_bytes(r3.at[s, 0:7], recv3.at[s])
         total = r3[s, 0].astype(F32)
         for i in range(1, NZ):
             total = total + r3[s, i].astype(F32)
-        row = lax.broadcasted_iota(jnp.int32, (128, BLOCK), 0)
-        col = lax.broadcasted_iota(jnp.int32, (128, BLOCK), 1)
+        row = lax.broadcasted_iota(jnp.int32, (64, SHARE), 0)
+        col = lax.broadcasted_iota(jnp.int32, (64, SHARE), 1)
         within = lax.rem(row, 16)
         pick = ((col == (row // 16) * 12 + within) & (within < 12)).astype(BF)
-        s4[s] = jnp.dot(pick, total.astype(BF), preferred_element_type=F32).astype(BF)
-        at = pl.multiple_of(LANES * s + BY_CORE * c + BY_X * x, BY_X)
-        for off in range(1, NX * NC):
-            j = lax.rem(me + off, NX * NC)
+        got = jnp.dot(pick, total.astype(BF), preferred_element_type=F32).astype(BF)
+        for i in range(4):
+            s4[s, i] = got[16 * i : 16 * (i + 1)]
+        lanes = pl.ds(pl.multiple_of(PIECE * s + BY_X * x, BY_X), BY_X)
+
+        def give(i):
+            j = 4 * c + i
             send(
-                s4.at[s, pl.ds(pl.multiple_of(16 * j, 16), 16), :], r4.at[:, pl.ds(at, BY_X)],
-                send4.at[s], recv4.at[s], {"fs_1": j // 2, "fs_2": lax.rem(j, 2)},
+                s4.at[s, i], r4.at[:, lanes], send4.at[s], recv4.at[s],
+                {"fs_1": j // 2, "fs_2": lax.rem(j, 2)},
             )
-        r4[:, pl.ds(at, BY_X)] = s4[s, pl.ds(pl.multiple_of(16 * me, 16), 16), :]
-
-    for q in range(NQ):
-        m, el = CHUNKS[q]
-        if q in (0, 1, 4):
-            reads[m].wait()
-        pack(q)
+
+        first = lax.rem(me, 4)
+        for step in range(1, 4):
+            give(lax.rem(first + step, 4))
+
+        @pl.when(amid)
+        def _():
+            r4[:, lanes] = s4[s, first]
+
+        @pl.when(jnp.logical_not(amid))
+        def _():
+            give(first)
+
+    def wait_rows(s, sem):
+        @pl.when(amid)
+        def _():
+            wait_bytes(r4.at[:, 0 : 3 * BY_X], sem.at[s])
+
+        @pl.when(jnp.logical_not(amid))
+        def _():
+            wait_bytes(r4.at[:, 0 : 4 * BY_X], sem.at[s])
+
+    pack(0)
     pl.semaphore_wait(barrier, len(peers))
     names = dict(
-        A=over_planes, R=relay, X=over_x, Z=over_z, S=spread, F=spread_on, P=arrived, N=normalize, H=hide,
+        K=pack, A=over_planes, R=relay, X=over_x, Z=over_z, Q=spread_first, S=spread, F=spread_on, P=arrived, N=normalize, H=hide,
         T=spread_down, U=spread_down_on, V=arrived_down,
         B=between_cores, C=sum_x, D=sum_x_on, E=sum_z, G=give_rows,
     )
@@ -315,7 +354,7 @@
         wait_bytes(w.at[q, 0:2], c_send.at[q])
         wait_bytes(w.at[q, 0], g_send.at[q])
         wait_bytes(w.at[q], o_sem.at[q])
-    for p in range(PIECES):
+    for p in range(PASSES):
         wait_bytes(w.at[4, :, :, 0:PIECE], c_send.at[4 + p])
         wait_bytes(piece(p, 0), g_send.at[4 + p])
         wait_bytes(w.at[4:6, :, :, 0:PIECE], o_sem.at[4 + p])
@@ -325,14 +364,11 @@
             wait_bytes(pb.at[i], send1.at[i])
             wait_bytes(t2.at[i], sendt.at[i])
             wait_bytes(r2.at[i], send2.at[i])
-            if PAIRS[k] == 0:
-                wait_bytes(s2.at[i, 0], send3.at[i])
-            else:
-                wait_bytes(s2.at[i], send3.at[i])
-        wait_bytes(r4.at[:, 0 : 7 * BY_X], recv4.at[s])
+            wait_bytes(s2.at[i, k:4], send3.at[i])
+        wait_rows(s, recv4)
     out[...] = r4[0:12, :]
     for s in range(PASSES):
-        wait_bytes(r4.at[:, 0 : 7 * BY_X], send4.at[s])
+        wait_rows(s, send4)
 
 
 def run(*args):
@@ -343,9 +379,12 @@
     return pl.pallas_call(
         kernel,
         out_shape=(weights, weights, weights, jax.ShapeDtypeStruct((12, WIDTH), BF)),
-        in_specs=[hbm, vmem, vmem, vmem, hbm, hbm, hbm],
+        in_specs=[hbm] * 7,
         out_specs=(hbm, hbm, hbm, vmem),
         scratch_shapes=[
+            pltpu.VMEM((2, ROWS), jnp.int32),
+            pltpu.VMEM((2, ROWS), F32),
+            pltpu.VMEM((1, 32), F32),
             pltpu.VMEM((3, 8, 32, 1024), F32),
             pltpu.VMEM((ROWS, WIDTH), BF),
             pltpu.VMEM((NQ, NY, 8, 32, 128), BF),
@@ -356,26 +395,26 @@
             pltpu.VMEM((NQ, NY, 64, WIDTH), BF),
             pltpu.VMEM((ROWS, WIDTH), BF),
             pltpu.VMEM((ROWS, 8), F32),
-            pltpu.VMEM((ROWS, 512), BF),
-            pltpu.VMEM((PASSES * NP, 2 * BLOCK, BY_CORE), BF),
-            pltpu.VMEM((PASSES * NP, 2 * BLOCK, BY_CORE), F32),
-            pltpu.VMEM((PASSES * NP, 2 * BLOCK, BY_CORE), BF),
+            pltpu.VMEM((NC, ROWS // NC, 512), BF),
+            pltpu.VMEM((PASSES * NP, PART, PIECE), BF),
+            pltpu.VMEM((PASSES * NP, PART, PIECE), F32),
+            pltpu.VMEM((PASSES * NP, PART, PIECE), BF),
             pltpu.VMEM((PASSES * NP, NX, 2, BLOCK, BY_X), BF),
             pltpu.VMEM((PASSES * NP, 2, BLOCK, BY_X), BF),
             pltpu.VMEM((PASSES * NP, 2, BLOCK, BY_X), BF),
             pltpu.VMEM((PASSES * NP, 2, 2, BLOCK, BY_X), BF),
-            pltpu.VMEM((PASSES * NP, 2, BLOCK, BY_X), BF),
-            pltpu.VMEM((PASSES, NZ, BLOCK, BY_X), BF),
-            pltpu.VMEM((PASSES, 128, BY_X), BF),
+            pltpu.VMEM((PASSES * NP, 4, SHARE, BY_X), BF),
+            pltpu.VMEM((PASSES, NZ, SHARE, BY_X), BF),
+            pltpu.VMEM((PASSES, 4, 16, BY_X), BF),
             pltpu.VMEM((16, WIDTH), BF),
-            dma((4,)),
+            dma((7,)),
             dma((NQ,)), dma((NQ,)),
             dma((NQ,)), dma((NQ, 2)),
             dma((NQ,)), dma((NQ,)),
-            dma((NQ,)), dma((NQ,)),
-            dma((4 + PIECES,)), dma((4 + PIECES, 2)),
-            dma((4 + PIECES,)), dma((4 + PIECES,)),
-            dma((4 + PIECES,)),
+            dma((NQ,)), dma((NQ,)), dma((EARLY, NZ)),
+            dma((4 + PASSES,)), dma((4 + PASSES, 2)),
+            dma((4 + PASSES,)), dma((4 + PASSES,)),
+            dma((4 + PASSES,)),
             dma((PASSES * NP,)), dma((PASSES * NP,)),
             dma((PASSES * NP,)), dma((PASSES * NP,)),
             dma((PASSES * NP,)), dma((PASSES * NP, 2)),

time: 120 us -> 114 us (0.950)
  Pallas kernels: 119 us -> 113 us
    pallas_call x1, Pallas kernels: 113 us -> 107 us  [run(): pl.pallas_call(kernel, out_shape=(weights, weights, weights, jax.ShapeDty...]
where the time goes in v3:
time: 114 us
  Pallas kernels  113 us (99%)
    pallas_call x1, Pallas kernels, run(): pl.pallas_call(kernel, out_shape=(weights, weights, weights, jax.ShapeDty...  107 us
    pallas_call x1, Pallas kernels, put_out(): pl.pallas_call(put_kernel, out_shape=(weights, weights, weights, small),...  5.54 us

profile of v3, /device:TPU:1, one launch (start us, length us, event | category | flops | bytes accessed | tf_op | source)
XLA Modules:
  0.0 113.7 jit_solution(4834528214824404961)
XLA Ops:
  0.6 107.5 %hand_over_and_serve.1 = (bf16[8,64,2048]{2,1,0:T(8,128)(2,1)}, bf16[8,64,2048]{2,1,0:T(8,128)(2,1)}, bf16[8,64,2048]{2,1,0:T(8,128)(2,1)}, bf16[12,2048]{1,0:T(8,128)(2,1)}) custom-call(bf16[768,2048]{1,0:T(8,128)(2,1)} %bitcast.12, s32[2,768]{1,0:T(2,128)} %bitcast.13, f32[2,768]{1,0:T(2,128)} %bitcast.14, f32[1,32]{1,0:T(1,128)} %bitcast.15, ...), custom_call_target="tpu_custom_call" | custom-call | tf_op jit(solution)/shard_map/hand_over_and_serve/pallas_call | solution.py:379
  108.1 5.5 %put_out.1 = (bf16[8,64,2048]{2,1,0:T(8,128)(2,1)}, bf16[8,64,2048]{2,1,0:T(8,128)(2,1)}, bf16[8,64,2048]{2,1,0:T(8,128)(2,1)}, bf16[12,2048]{1,0:T(8,128)(2,1)}) custom-call(bf16[8,64,2048]{2,1,0:T(8,128)(2,1)} %get-tuple-element.12.wg, bf16[8,64,2048]{2,1,0:T(8,128)(2,1)} %get-tuple-element.13.wu, bf16[8,64,2048]{2,1,0:T(8,128)(2,1)} %get-tuple-element.14.wd, ...), custom_call_target="tpu_custom_call" | custom-call | tf_op jit(solution)/shard_map/put_out/pallas_call | solution.py:452

commit v4 on v3

--- a/solution.py
+++ b/solution.py
@@ -16,7 +16,7 @@
 NQ = len(CHUNKS)
 ROWS, WIDTH = 768, 2048
 BLOCK = ROWS // NZ
-EARLY = 2
+EARLY = 3
 PASSES = 4
 PIECE = WIDTH // PASSES
 BY_X = PIECE // NX
@@ -24,12 +24,12 @@
 PART = ROWS // NC // NP
 SHARE = BLOCK // NC
 ORDER = (
-    "A0 K1 A1 K2", "K3 K4 K5 R0", "A2 X0 R1 A3", "R2", "X1 A4 R3 X2", "Z0 A5 Q0,0 R4",
+    "A0 K1 K2 K3", "R0 A1 K4 K5", "A2 X0 R1 A3", "R2", "X1 A4 R3 X2", "Z0 A5 Q0,0 R4",
     "X3 Q0,1 Q0,7 Z1", "R5 Q1,0 X4 Q0,2", "Q0,6 X5 Z2 Q1,1", "Q1,7 Q0,3 Q0,5 N0",
-    "Z3 Q1,2 Q1,6 N1", "Q0,4 Z4 N2 N3", "Q1,3 Q1,5 F0", "Z5 N4 N5",
-    "Q1,4 N6 N7", "S2 N8 F1", "N9 N10 N11 P0",
-    "S3 F2 P1", "H0,0 H0,1", "F3 T0 T1 P2", "P3 H1,0 H1,1",
-    "U0 T2 U1 T3", "V0 B0,0 B0,1 U2", "C0,0 C0,1 V1 B1,0",
+    "Z3 Q1,2 Q1,6 N1", "Q0,4 Z4 N2 N3", "Q1,3 Q1,5 F0", "Z5 Q2,0 N4 N5",
+    "Q1,4 Q2,1 Q2,7 N6", "Q2,2 Q2,6 N7 N8", "Q2,3 Q2,5 N9 N10", "F1 Q2,4 N11 P0",
+    "S3 F2 P1", "H0,0 H0,1", "F3 T0 T1 P2", "P3 H1,0 U0 T2",
+    "H1,1 U1 T3", "V0 B0,0 B0,1 U2", "C0,0 C0,1 V1 B1,0",
     "B1,1 U3 D0,0 C1,0", "D0,1 C1,1 V2", "B2,0 B2,1 E0,0 V3",
     "B3,0 B3,1 D1,0 E0,1", "C2,0 D1,1 C2,1 C3,0", "C3,1 E1,0 D2,0 G0",
     "E1,1 D2,1 D3,0 D3,1", "E2,0 G1 E2,1 E3,0", "E3,1 G2 G3",
@@ -422,25 +422,21 @@
             dma((PASSES,)), dma((PASSES,)),
         ],
         compiler_params=pltpu.CompilerParams(
-            collective_id=0, has_side_effects=True, vmem_limit_bytes=60 * 1024 * 1024
+            collective_id=0, has_side_effects=True, vmem_limit_bytes=40 * 1024 * 1024
         ),
         name="hand_over_and_serve",
     )(*args)
 
 
-def put_kernel(wg, wu, wd, small, og, ou, od, out, buf, buf_small, sems):
-    hops = [(small, buf_small, out)]
-    for m, (w, o) in enumerate(((wg, og), (wu, ou), (wd, od))):
+def put_kernel(wg, wu, wd, small, og, ou, od, out, sems):
+    hops = [(small, out)]
+    for w, o in ((wg, og), (wu, ou), (wd, od)):
         for i in range(4):
             two = slice(2 * i, 2 * i + 2)
-            hops.append((w.at[two], buf.at[m, two], o.at[two]))
-    reads = [pltpu.make_async_copy(a, b, sems.at[0, n]) for n, (a, b, _) in enumerate(hops)]
-    writes = [pltpu.make_async_copy(b, o, sems.at[1, n]) for n, (_, b, o) in enumerate(hops)]
-    for copy in reads:
+            hops.append((w.at[two], o.at[two]))
+    writes = [pltpu.make_async_copy(a, o, sems.at[n]) for n, (a, o) in enumerate(hops)]
+    for copy in writes:
         copy.start()
-    for read, write in zip(reads, writes):
-        read.wait()
-        write.start()
     for copy in writes:
         copy.wait()
 
@@ -449,26 +445,24 @@
     weights = jax.ShapeDtypeStruct((8, 64, WIDTH), BF)
     small = jax.ShapeDtypeStruct((12, WIDTH), BF)
     hbm = pl.BlockSpec(memory_space=pl.ANY)
+    vmem = pl.BlockSpec(memory_space=pltpu.VMEM)
     return pl.pallas_call(
         put_kernel,
         out_shape=(weights, weights, weights, small),
-        in_specs=[hbm] * 4,
+        in_specs=[vmem] * 4,
         out_specs=(hbm, hbm, hbm, hbm),
-        scratch_shapes=[
-            pltpu.VMEM((3, 8, 64, WIDTH), BF),
-            pltpu.VMEM((12, WIDTH), BF),
-            pltpu.SemaphoreType.DMA((2, 13)),
-        ],
-        compiler_params=pltpu.CompilerParams(vmem_limit_bytes=60 * 1024 * 1024),
+        scratch_shapes=[pltpu.SemaphoreType.DMA((13,))],
+        compiler_params=pltpu.CompilerParams(vmem_limit_bytes=16 * 1024 * 1024),
         name="put_out",
     )(*results)
 
 
 def local(tokens, norm_gain, gate_weight, up_weight, down_weight, expert_ids, expert_mix):
-    results = run(
+    args = (
         tokens.reshape(ROWS, WIDTH), expert_ids.reshape(ROWS, 2).T, expert_mix.reshape(ROWS, 2).T,
         norm_gain.reshape(1, 32), gate_weight, up_weight, down_weight,
     )
+    results = run(*(pltpu.with_memory_space_constraint(a, pltpu.HBM) for a in args))
     gate_t, up_t, down_t, mixed = put_out(*results)
     turned = tuple(jnp.swapaxes(t, 1, 2) for t in (gate_t, up_t, down_t))
     return turned + (mixed.reshape(12, 1, WIDTH),)

time: 114 us -> 109 us (0.956)
  Pallas kernels: 113 us -> 109 us
    pallas_call x1, Pallas kernels: 5.54 us -> 2.78 us  [put_out(): pl.pallas_call(put_kernel, out_shape=(weights, weights, weights, small),...]
    pallas_call x1, Pallas kernels: 107 us -> 106 us  [run(): pl.pallas_call(kernel, out_shape=(weights, weights, weights, jax.ShapeDty...]
where the time goes in v4:
time: 109 us
  Pallas kernels  109 us (100%)
    pallas_call x1, Pallas kernels, run(): pl.pallas_call(kernel, out_shape=(weights, weights, weights, jax.ShapeDty...  106 us
    pallas_call x1, Pallas kernels, put_out(): pl.pallas_call(put_kernel, out_shape=(weights, weights, weights, small),...  2.78 us

profile of v4, /device:TPU:1, one launch (start us, length us, event | category | flops | bytes accessed | tf_op | source)
XLA Modules:
  0.0 109.4 jit_solution(15885539193846959231)
XLA Ops:
  0.6 106.0 %hand_over_and_serve.1 = (bf16[8,64,2048]{2,1,0:T(8,128)(2,1)S(1)}, bf16[8,64,2048]{2,1,0:T(8,128)(2,1)S(1)}, bf16[8,64,2048]{2,1,0:T(8,128)(2,1)S(1)}, bf16[12,2048]{1,0:T(8,128)(2,1)S(1)}) custom-call(bf16[768,2048]{1,0:T(8,128)(2,1)} %bitcast.12, s32[2,768]{1,0:T(2,128)} %bitcast.13, f32[2,768]{1,0:T(2,128)} %bitcast.14, f32[1,32]{1,0:T(1,128)} %bitcast.15, ...), custom_call_target="tpu_custom_call" | custom-call | tf_op jit(solution)/shard_map/hand_over_and_serve/pallas_call | solution.py:379
  106.6 2.8 %put_out.1 = (bf16[8,64,2048]{2,1,0:T(8,128)(2,1)}, bf16[8,64,2048]{2,1,0:T(8,128)(2,1)}, bf16[8,64,2048]{2,1,0:T(8,128)(2,1)}, bf16[12,2048]{1,0:T(8,128)(2,1)}) custom-call(bf16[8,64,2048]{2,1,0:T(8,128)(2,1)S(1)} %get-tuple-element.12.wg, bf16[8,64,2048]{2,1,0:T(8,128)(2,1)S(1)} %get-tuple-element.13.wu, bf16[8,64,2048]{2,1,0:T(8,128)(2,1)S(1)} %get-tuple-element.14.wd, ...), custom_call_target="tpu_custom_call" | custom-call | tf_op jit(solution)/shard_map/put_out/pallas_call | solution.py:449

commit v5 on v4

--- a/solution.py
+++ b/solution.py
@@ -63,7 +63,7 @@
 
     pairs = ((gain_in, gain), (gate, mat.at[0]), (up, mat.at[1]), (down, mat.at[2]), (tokens, tok), (ids_in, ids), (mix_in, mix))
     reads = [pltpu.make_async_copy(src, dst, in_sem.at[n]) for n, (src, dst) in enumerate(pairs)]
-    for r in reads:
+    for r in reads[:2]:
         r.start()
 
     barrier = pltpu.get_barrier_semaphore()
@@ -83,6 +83,9 @@
             reads[0].wait()
         if el == 0:
             reads[1 + m].wait()
+        if q == 0:
+            for r in reads[2:]:
+                r.start()
         low = lax.broadcasted_iota(jnp.int32, (32, 128), 1) < 64
         eye = lax.broadcasted_iota(jnp.int32, (32, 32), 0) == lax.broadcasted_iota(jnp.int32, (32, 32), 1)
         scale = jnp.sum(jnp.where(eye, gain[...], 0.0), axis=1, keepdims=True)

time: 109 us -> 109 us (level)
  no operation moved by 1% of the time
where the time goes in v5:
time: 109 us
  Pallas kernels  109 us (100%)
    pallas_call x1, Pallas kernels, run(): pl.pallas_call(kernel, out_shape=(weights, weights, weights, jax.ShapeDty...  106 us
    pallas_call x1, Pallas kernels, put_out(): pl.pallas_call(put_kernel, out_shape=(weights, weights, weights, small),...  2.78 us

profile of v5, /device:TPU:1, one launch (start us, length us, event | category | flops | bytes accessed | tf_op | source)
XLA Modules:
  0.0 109.4 jit_solution(7710373265814859838)
XLA Ops:
  0.6 106.0 %hand_over_and_serve.1 = (bf16[8,64,2048]{2,1,0:T(8,128)(2,1)S(1)}, bf16[8,64,2048]{2,1,0:T(8,128)(2,1)S(1)}, bf16[8,64,2048]{2,1,0:T(8,128)(2,1)S(1)}, bf16[12,2048]{1,0:T(8,128)(2,1)S(1)}) custom-call(bf16[768,2048]{1,0:T(8,128)(2,1)} %bitcast.12, s32[2,768]{1,0:T(2,128)} %bitcast.13, f32[2,768]{1,0:T(2,128)} %bitcast.14, f32[1,32]{1,0:T(1,128)} %bitcast.15, ...), custom_call_target="tpu_custom_call" | custom-call | tf_op jit(solution)/shard_map/hand_over_and_serve/pallas_call | solution.py:382
  106.6 2.8 %put_out.1 = (bf16[8,64,2048]{2,1,0:T(8,128)(2,1)}, bf16[8,64,2048]{2,1,0:T(8,128)(2,1)}, bf16[8,64,2048]{2,1,0:T(8,128)(2,1)}, bf16[12,2048]{1,0:T(8,128)(2,1)}) custom-call(bf16[8,64,2048]{2,1,0:T(8,128)(2,1)S(1)} %get-tuple-element.12.wg, bf16[8,64,2048]{2,1,0:T(8,128)(2,1)S(1)} %get-tuple-element.13.wu, bf16[8,64,2048]{2,1,0:T(8,128)(2,1)S(1)} %get-tuple-element.14.wd, ...), custom_call_target="tpu_custom_call" | custom-call | tf_op jit(solution)/shard_map/put_out/pallas_call | solution.py:452
